TPU v7x, 512 devices: a whole 4x8x8 slice. The times are simulated.
512 devices in a mesh: dp: 4 (over x), kv: 64 (over z, y), tp: 2 (over core).
Axes of the slice: x: 4, y: 8, z: 8, core: 2. Of those that a mesh axis runs over, the one named last changes fastest.
Arguments:
- tokens: bfloat16 [131072, 2048], P(('dp', 'kv')), parts along dimension 0, may hold values from -60 to 60, as said below
- chosen: int32 [2048, 16], P(('dp', 'kv')), parts along dimension 0, may hold values from -1 to 511, as said below
- query_weight: bfloat16 [2048, 1024], P('kv', 'tp'), may hold values from -0.125 to 0.125
- key_matrix: bfloat16 [2048, 128], P('kv', 'tp'), may hold values from -0.125 to 0.125
- value_matrix: bfloat16 [2048, 128], P('kv', 'tp'), may hold values from -0.125 to 0.125
- out_weight: bfloat16 [1024, 2048], P('tp', 'kv'), may hold values from -0.1875 to 0.1875
- out_gain: float32 [2048], replicated, may hold values from 0.1 to 1.9
Outputs:
- mixed_out: bfloat16 [131072, 2048], P(('dp', 'kv', 'tp')), parts along dimension 0
There are 4 independent parts, one for each index of `dp`. A program takes and returns all parts, laid end to end along the dimension named above; an argument that names none is the same for every part. Nothing has to cross between parts.
Inputs may be any that keep to these rules, and one draw needn't show every extreme that they name: tokens are of order one apart from few rows. chosen[g, 0] = g; every other entry of row g is -1 or a block below g, and the entries of a row other than -1 are distinct; the blocks that the rows of one device name on any single other device are at most 2 different ones, and this is reached.
All inputs are finite; a program needn't handle non-finite values.
Results may differ from a plain program's by a relative error of at most 0.012.
The roundings to bfloat16 on the way count: a program that leaves them out, or rounds other values in their place, can miss the bound.
Values may be sent and summed in bfloat16 or wider, within the bound.
A program may use at most 64 MiB of HBM per device.

v0:
```python
import jax
import jax.numpy as jnp
from jax import lax
from jax.sharding import PartitionSpec as P

HEAD_WIDTH = 64
BLOCK_LENGTH = 64
CAP = 2


def side_by_side(arrays, axis, dim, along):
    both = jnp.concatenate(arrays, axis=along)
    filled, at, gathered = (lax.all_gather(both, axis, axis=dim, tiled=True), 0, [])
    for a in arrays:
        gathered.append(lax.slice_in_dim(filled, at, at + a.shape[along], axis=along))
        at += a.shape[along]
    return tuple(gathered)


def split_up(shard, dim, length):
    dims = shard.shape
    tiles = shard.reshape(*dims[:dim], length, dims[dim] // length, *dims[dim + 1 :])
    return jnp.moveaxis(tiles, dim, 0)


def summed_on_arrival(shard, axis, dim):
    tiles = split_up(shard, dim, lax.axis_size(axis))
    arrived = lax.all_to_all(tiles, axis, split_axis=0, concat_axis=0, tiled=True)
    return arrived.astype(jnp.float32).sum(axis=0)


def per_device(tokens, chosen, query_weight, key_matrix, value_matrix, out_weight, out_gain):
    tok_rows = tokens.shape[0]
    blocks = tok_rows // BLOCK_LENGTH
    device = lax.axis_index("kv")
    kv_count = lax.axis_size("kv")
    whole_query, whole_key, whole_value = side_by_side(
        (query_weight, key_matrix, value_matrix), "kv", 0, 1
    )
    query_rows = jnp.dot(tokens, whole_query, preferred_element_type=jnp.float32).astype(
        jnp.bfloat16
    )
    key_rows = jnp.dot(tokens, whole_key, preferred_element_type=jnp.float32).astype(jnp.bfloat16)
    value_rows = jnp.dot(tokens, whole_value, preferred_element_type=jnp.float32).astype(
        jnp.bfloat16
    )
    paired = jnp.concatenate([key_rows, value_rows], axis=1)
    pair_width = paired.shape[1]
    own_blocks = paired.reshape(blocks, BLOCK_LENGTH, pair_width)
    safe_ids = jnp.maximum(chosen, 0)
    owner_dev = safe_ids // blocks
    offset = safe_ids - owner_dev * blocks
    remote = (chosen >= 0) & (owner_dev != device)
    targets = jnp.arange(kv_count * blocks, dtype=jnp.int32)
    wanted = jnp.any(
        (safe_ids.reshape(-1, 1) == targets[None, :]) & remote.reshape(-1, 1), axis=0
    ).reshape(kv_count, blocks)
    slot_rank = jnp.cumsum(wanted.astype(jnp.int32), axis=1) - 1
    slot_index = jnp.arange(CAP, dtype=jnp.int32)
    matches = wanted[:, :, None] & (slot_rank[:, :, None] == slot_index[None, None, :])
    requests = jnp.sum(
        jnp.where(matches, jnp.arange(blocks, dtype=jnp.int32)[None, :, None], 0), axis=1
    )
    fetched = jnp.take(
        own_blocks, lax.all_to_all(requests, "kv", split_axis=0, concat_axis=0, tiled=True), axis=0
    )
    received = lax.all_to_all(fetched, "kv", split_axis=0, concat_axis=0, tiled=True)
    slot_found = jnp.take(slot_rank.reshape(-1), safe_ids)
    placed = jnp.where(
        owner_dev == device, offset, blocks + owner_dev * CAP + jnp.clip(slot_found, 0, CAP - 1)
    )
    block_pool = jnp.concatenate(
        [own_blocks, received.reshape(-1, BLOCK_LENGTH, pair_width)], axis=0
    )
    picked = jnp.take(block_pool, placed, axis=0)
    head_count = query_rows.shape[1] // HEAD_WIDTH
    grouped = query_rows.reshape(blocks, BLOCK_LENGTH, head_count, HEAD_WIDTH)
    offsets = jnp.arange(BLOCK_LENGTH, dtype=jnp.int32)
    query_pos = (device * blocks + jnp.arange(blocks, dtype=jnp.int32))[
        :, None
    ] * BLOCK_LENGTH + offsets[None, :]
    key_pos = safe_ids[:, :, None] * BLOCK_LENGTH + offsets[None, None, :]
    visible = (chosen >= 0)[:, None, :, None] & (
        key_pos[:, None, :, :] <= query_pos[:, :, None, None]
    )

    def attend_block(inputs):
        query_block, pair_block, seen = inputs
        block_keys = pair_block[..., :HEAD_WIDTH]
        block_values = pair_block[..., HEAD_WIDTH:]
        scores = jnp.einsum(
            "qgd,skd->gqsk", query_block, block_keys, preferred_element_type=jnp.float32
        ) * HEAD_WIDTH ** (-0.5)
        scores = jnp.where(seen[None], scores, -1e30)
        row_max = jnp.max(scores, axis=(2, 3), keepdims=True)
        expon = jnp.exp(scores - row_max)
        row_sum = jnp.sum(expon, axis=(2, 3), keepdims=True)
        weights_bf = (expon / row_sum).astype(jnp.bfloat16)
        result = jnp.einsum(
            "gqsk,skd->qgd", weights_bf, block_values, preferred_element_type=jnp.float32
        )
        return result.astype(jnp.bfloat16)

    attended = lax.map(attend_block, (grouped, picked, visible))
    attended = attended.reshape(tok_rows, head_count * HEAD_WIDTH)
    whole_out = lax.all_gather(out_weight, "kv", axis=1, tiled=True)
    mixed = summed_on_arrival(
        jnp.dot(attended, whole_out, preferred_element_type=jnp.float32).astype(jnp.bfloat16),
        "tp",
        0,
    )
    normed = mixed * lax.rsqrt(jnp.mean(mixed * mixed, axis=-1, keepdims=True) + 1e-06) * out_gain
    return normed.astype(jnp.bfloat16)


def solution(mesh):
    placed = (
        P(("dp", "kv"), None),
        P(("dp", "kv"), None),
        P("kv", "tp"),
        P("kv", "tp"),
        P("kv", "tp"),
        P("tp", "kv"),
        P(),
    )
    return jax.shard_map(
        per_device,
        mesh=mesh,
        in_specs=placed,
        out_specs=P(("dp", "kv", "tp"), None),
        check_vma=False,
    )
```

profile of v0, /device:TPU:1, one launch (start us, length us, event | category | flops | bytes accessed | tf_op | source)
XLA Modules:
  0.0 245.8 jit_solution(11396263107951894309)
XLA Ops:
  6.5 1.6 pad_maximum_fusion.2
  10.5 27.8 %all_to_all.25 = s32[64,1,2]{2,1,0:T(1,128)S(1)} all-to-all(s32[64,1,2]{2,1,0:T(1,128)S(1)} %copy.35), channel_id=1, replica_groups=mesh['dp'=4,'kv'=64,'tp'=2] {'kv'}, dimensions={0} | all-to-all | bytes 1024 | tf_op jit(solution)/shard_map/all_to_all | solution.py:65
  38.7 57.5 %all-gather.3.cloned.1.call-done = bf16[2048,640]{1,0:T(8,128)(2,1)} async-done(((bf16[32,640]{1,0:T(8,128)(2,1)}), bf16[2048,640]{1,0:T(8,128)(2,1)}) %all-gather.3.cloned.1.call-update) | async-done | bytes 2621456 | tf_op jit(solution)/shard_map/all_gather | solution.py:13
  96.2 1.8 fusion.20
  98.1 2.1 fusion.21
  100.3 2.1 gather_fusion.1
  102.5 3.2 %broadcast_select_fusion = bf16[64,2,64,128]{3,2,1,0:T(8,128)(2,1)} fusion(bf16[64,2,64,128]{3,2,1,0:T(8,128)(2,1)} %bitcast.100, pred[64,2]{1,0:T(8,128)(4,1)S(1)} %copy.37), kind=kLoop, calls=%fused_computation.31 | loop fusion | flops 1048576 | bytes 4194432 | tf_op jit(solution)/shard_map/jit(_take)/select_n | solution.py:64
  105.7 8.6 %all-to-all-start.1 = ((bf16[64,2,64,128]{3,2,1,0:T(8,128)(2,1)}), bf16[64,2,64,128]{3,2,1,0:T(8,128)(2,1)}, u32[]{:S(2)}, u32[]{:S(2)}) async-start(bf16[64,2,64,128]{3,2,1,0:T(8,128)(2,1)} %broadcast_select_fusion), calls=%async_computation.1 | async-start | bytes 4194304 | tf_op jit(solution)/shard_map/all_to_all | solution.py:67
  115.2 1.3 gather_fusion
  116.8 2.6 %compare_and_fusion = pred[8,64,16,64]{1,3,2,0:T(8,128)(4,1)} fusion(s32[8,64]{1,0:T(8,128)S(1)} %iota_add_fusion.1, s32[8,16,64]{2,1,0:T(8,128)S(1)} %iota_add_fusion, pred[8,16]{1,0:T(8,128)(4,1)S(1)} %get-tuple-element.66), kind=kLoop, calls=%fused_computation.24 | loop fusion | flops 1048576 | bytes 559232 | tf_op jit(solution)/shard_map/and | solution.py:83
  119.4 3.7 %fusion.17 = bf16[512,512]{0,1:T(8,128)(2,1)} fusion(bf16[512,2048]{1,0:T(8,128)(2,1)S(1)} %copy-done, bf16[2048,640]{1,0:T(8,128)(2,1)} %all-gather.3.cloned.1.call-done), kind=kOutput, calls=%fused_computation.34 | convolution fusion | flops 1074003968 | bytes 4718592 | tf_op jit(solution)/shard_map/dot_general | solution.py:40
  123.1 1.6 reshape.122
  124.7 1.6 copy.40
  126.3 32.7 %all-to-all-done.1 = bf16[64,2,64,128]{3,2,1,0:T(8,128)(2,1)} async-done(((bf16[64,2,64,128]{3,2,1,0:T(8,128)(2,1)}), bf16[64,2,64,128]{3,2,1,0:T(8,128)(2,1)}, u32[]{:S(2)}, u32[]{:S(2)}) %all-to-all-start.1) | async-done | bytes 2097184 | tf_op jit(solution)/shard_map/all_to_all | solution.py:67
  159.1 3.2 %pad_maximum_fusion = bf16[136,64,128]{2,1,0:T(8,128)(2,1)} fusion(bf16[128,64,128]{2,1,0:T(8,128)(2,1)} %bitcast.19, bf16[8,64,128]{2,1,0:T(8,128)(2,1)S(1)} %bitcast.98), kind=kLoop, calls=%fused_computation.26 | loop fusion | flops 1114112 | bytes 4456448 | tf_op jit(solution)/shard_map/concatenate | solution.py:72
  162.2 3.8 %gather_fusion.2 = bf16[128,64,128]{2,1,0:T(8,128)(2,1)} fusion(bf16[136,64,128]{2,1,0:T(8,128)(2,1)} %pad_maximum_fusion, s32[1024]{0:T(1024)S(1)} %pad_clamp_fusion), kind=kCustom, calls=%fused_computation.2 | custom fusion | bytes 4194816 | tf_op jit(solution)/shard_map/jit(_take)/gather | solution.py:75
  166.0 3.3 %broadcast_select_fusion.1 = bf16[8,16,64,128]{3,2,1,0:T(8,128)(2,1)} fusion(bf16[8,16,64,128]{3,2,1,0:T(8,128)(2,1)} %bitcast.99, pred[8,16]{1,0:T(8,128)(4,1)S(1)} %get-tuple-element.63), kind=kLoop, calls=%fused_computation.32 | loop fusion | flops 1048576 | bytes 4194432 | tf_op jit(solution)/shard_map/jit(_take)/select_n | solution.py:75
  169.3 49.3 %while.10 = (s32[]{:T(128)}, bf16[8,64,8,64]{3,2,1,0:T(8,128)(2,1)S(1)}, bf16[8,16,64,128]{3,2,1,0:T(8,128)(2,1)}, pred[8,64,16,64]{1,3,2,0:T(8,128)(4,1)}, bf16[8,64,8,64]{3,1,2,0:T(8,128)(2,1)}, /*index=5*/s32[]{:T(128)}) while((s32[]{:T(128)}, bf16[8,64,8,64]{3,2,1,0:T(8,128)(2,1)S(1)}, bf16[8,16,64,128]{3,2,1,0:T(8,128)(2,1)}, ...), condition=%wide.region_6.7_spmd, body=%wide.region_3.6_spmd.sunk | while | flops 140540928 | bytes 8268369 | solution.py:104
  171.2 1.8 fusion.36
  174.1 1.2 fusion.38
  177.4 1.8 fusion.36
  183.6 1.8 fusion.36
  189.7 1.8 fusion.36
  195.9 1.8 fusion.36
  198.7 1.2 fusion.38
  202.1 1.8 fusion.36
  208.2 1.8 fusion.36
  211.1 1.2 fusion.38
  214.4 1.8 fusion.36
  218.7 1.4 reshape.123
  220.1 3.0 %convolution_convert_fusion = bf16[512,2048]{1,0:T(8,128)(2,1)S(1)} fusion(bf16[512,512]{1,0:T(8,128)(2,1)} %reshape.123, bf16[512,2048]{0,1:T(8,128)(2,1)} %all-gather.5.cloned.1.call-done), kind=kOutput, calls=%fused_computation.25 | convolution fusion | flops 1074790400 | bytes 4718592 | tf_op jit(solution)/shard_map/dot_general | solution.py:108
  223.2 13.4 %all_to_all.26 = bf16[2,256,2048]{2,1,0:T(8,128)(2,1)S(1)} all-to-all(bf16[2,256,2048]{2,1,0:T(8,128)(2,1)S(1)} %bitcast.101), channel_id=1, replica_groups=mesh['dp'=4,'kv'=64,'tp'=2] {'tp'}, dimensions={0} | all-to-all | bytes 4194304 | tf_op jit(solution)/shard_map/all_to_all | solution.py:28
  (94 shorter events, 37.2 us)
Async XLA Ops:
  6.5 89.7 %copy-start = (bf16[512,2048]{1,0:T(8,128)(2,1)S(1)}, bf16[512,2048]{1,0:T(8,128)(2,1)}, u32[]{:S(2)}) copy-start(bf16[512,2048]{1,0:T(8,128)(2,1)} %param.9) | copy-start | bytes 6291460
  6.5 89.7 %all-gather.3.cloned.1.call-start = ((), (), s32[]{:S(2)}) async-start(), calls=%async_computation.3 | async-start | bytes 2662400 | tf_op jit(solution)/shard_map/all_gather | solution.py:13
  105.7 53.3 %all-to-all-start.1 = ((bf16[64,2,64,128]{3,2,1,0:T(8,128)(2,1)}), bf16[64,2,64,128]{3,2,1,0:T(8,128)(2,1)}, u32[]{:S(2)}, u32[]{:S(2)}) async-start(bf16[64,2,64,128]{3,2,1,0:T(8,128)(2,1)} %broadcast_select_fusion), calls=%async_computation.1 | async-start | bytes 4194304 | tf_op jit(solution)/shard_map/all_to_all | solution.py:67
  114.3 105.8 %all-gather.5.cloned.1.call-start = ((), (), s32[]{:S(2)}) async-start(), calls=%async_computation.4 | async-start | bytes 2129920 | tf_op jit(solution)/shard_map/all_gather | solution.py:106
  115.2 1.4 copy-start.2
  166.0 3.3 %copy-start.1 = (bf16[8,64,8,64]{3,2,1,0:T(8,128)(2,1)S(1)}, bf16[8,64,8,64]{3,2,1,0:T(8,128)(2,1)}, u32[]{:S(2)}) copy-start(bf16[8,64,8,64]{3,2,1,0:T(8,128)(2,1)} %custom-call.6) | copy-start | bytes 1572868
  237.1 0.7 copy-start.3
Sparse Core Ops, SparseCore 0:
  10.3 85.8 all-gather.2
  118.2 99.4 all-gather.4
where the time goes:
time: 247 us; the launch traced here: 246 us
  waiting for transfers between devices  90.8 us (37%)
  blocking collectives  41.2 us (17%)
  matrix products  35 us (14%)
  local copies, waits for them, and re-layouts  30.1 us (12%)
  other arithmetic  25.9 us (10%)
  between operations  13.6 us (6%)
  starting transfers between devices  8.8 us (4%)
    all_gather x1, waiting for transfers between devices, side_by_side(): lax.all_gather(both, axis, axis=dim, tiled=True)  57.5 us
    all_to_all x1, waiting for transfers between devices, per_device(): lax.all_to_all(fetched, 'kv', split_axis=0, concat_axis=0, tiled=True)  32.7 us
    all_to_all x1, blocking collectives, per_device(): lax.all_to_all(requests, 'kv', split_axis=0, concat_axis=0, tiled=True)  27.8 us
    dot_general x8, matrix products, attend_block(): jnp.einsum('qgd,skd->gqsk', query_block, block_keys, preferred_element_ty...  14.4 us
    all_to_all x1, blocking collectives, summed_on_arrival(): lax.all_to_all(tiles, axis, split_axis=0, concat_axis=0, tiled=True)  13.4 us
    dot_general x8, matrix products, attend_block(): jnp.einsum('gqsk,skd->qgd', weights_bf, block_values, preferred_element_t...  9.96 us
    all_to_all x1, starting transfers between devices, per_device(): lax.all_to_all(fetched, 'kv', split_axis=0, concat_axis=0, tiled=True)  8.57 us
    reduce_sum x8, other arithmetic, attend_block(): row_sum = jnp.sum(expon, axis=(2, 3), keepdims=True)  8.14 us
  transfers between devices with their start and end apart: 3, of which 2 were waited for; matrix products, arithmetic and copies ran while one was open for 30% of the time, Pallas kernels for 0%

commit v1 on v0

v1 whole, which is shorter than its diff:
```python
import functools

import jax
import jax.numpy as jnp
from jax import lax
from jax.experimental import pallas as pl
from jax.experimental.pallas import tpu as pltpu
from jax.sharding import PartitionSpec as P

HEAD_WIDTH = 64
BLOCK_LENGTH = 64
CAP = 2
NEG = -1e30
MESH = pl.DeviceIdType.MESH


def fused_kernel(
    dims,
    placed_ref,
    requests_ref,
    tokens_hbm,
    pair_ref,
    query_ref,
    out_ref,
    gain_ref,
    result_ref,
    tokens,
    pair_all,
    requests_all,
    requests_smem,
    query_all,
    out_all,
    own,
    pool,
    packed,
    queries,
    gathered,
    attended,
    part_mine,
    part_send,
    part_recv,
    tok_sem,
    smem_sem,
    pair_sem,
    request_sem,
    y_sem,
    ring_send,
    ring_recv,
    x_send,
    x_recv,
    block_send,
    block_recv,
    half_sem,
):
    n_dp, n_kv, n_y = dims
    n_z = n_kv // n_y
    dp, kv, tp = lax.axis_index("dp"), lax.axis_index("kv"), lax.axis_index("tp")
    z, y = kv // n_y, lax.rem(kv, n_y)
    depth = pair_ref.shape[0]
    blocks = own.shape[0]
    quarter = query_ref.shape[1] // n_dp

    def remote(src, dst, send, recv, to_dp, to_kv, to_tp):
        return pltpu.make_async_remote_copy(
            src_ref=src,
            dst_ref=dst,
            send_sem=send,
            recv_sem=recv,
            device_id=(to_dp, to_kv, to_tp),
            device_id_type=MESH,
        )

    load_tokens = pltpu.make_async_copy(tokens_hbm, tokens, tok_sem)
    load_tokens.start()

    barrier = pltpu.get_barrier_semaphore()

    def greet(off, carry):
        other = lax.rem(kv + off, n_kv)
        pl.semaphore_signal(barrier, inc=1, device_id=(dp, other, tp), device_id_type=MESH)
        return carry

    lax.fori_loop(1, n_kv, greet, 0)
    for off in range(1, n_dp):
        pl.semaphore_signal(
            barrier, inc=1, device_id=(lax.rem(dp + off, n_dp), kv, tp), device_id_type=MESH
        )
    pl.semaphore_signal(barrier, inc=1, device_id=(dp, kv, 1 - tp), device_id_type=MESH)

    my_rows = pl.ds(pl.multiple_of(kv * depth, depth), depth)
    my_cols = pl.ds(pl.multiple_of(dp * quarter, quarter), quarter)
    pair_all[my_rows, :] = pair_ref[...]
    query_all[my_rows, my_cols] = query_ref[:, my_cols]
    out_all[my_rows, my_cols] = out_ref[:, my_cols]

    pl.semaphore_wait(barrier, n_kv - 1 + n_dp - 1 + 1)

    def send_pair(off, carry):
        other = lax.rem(kv + off, n_kv)
        remote(
            pair_ref, pair_all.at[my_rows, :], pair_sem.at[0], pair_sem.at[1], dp, other, tp
        ).start()
        remote(
            requests_ref.at[pl.ds(other, 1)],
            requests_all.at[pl.ds(kv, 1)],
            request_sem.at[0],
            request_sem.at[1],
            dp,
            other,
            tp,
        ).start()
        return carry

    lax.fori_loop(1, n_kv, send_pair, 0)

    def send_row(off, carry):
        other = z * n_y + lax.rem(y + off, n_y)
        remote(
            query_ref.at[:, my_cols],
            query_all.at[my_rows, my_cols],
            y_sem.at[0],
            y_sem.at[1],
            dp,
            other,
            tp,
        ).start()
        remote(
            out_ref.at[:, my_cols],
            out_all.at[my_rows, my_cols],
            y_sem.at[2],
            y_sem.at[3],
            dp,
            other,
            tp,
        ).start()
        return carry

    lax.fori_loop(1, n_y, send_row, 0)

    def drain(ref, sem):
        pltpu.make_async_copy(ref, ref, sem).wait()

    others = pair_all.at[pl.ds(0, (n_kv - 1) * depth), :]
    drain(others, pair_sem.at[1])
    drain(requests_all.at[pl.ds(0, n_kv - 1)], request_sem.at[1])
    to_smem = pltpu.make_async_copy(requests_all, requests_smem, smem_sem)
    to_smem.start()
    load_tokens.wait()
    pairs = jnp.dot(tokens[...], pair_all[...], preferred_element_type=jnp.float32)
    pairs = pairs.astype(jnp.bfloat16).reshape(own.shape)
    own[...] = pairs
    pool[pl.ds(n_kv * CAP, blocks)] = pairs
    to_smem.wait()

    def block_copy(owner, to):
        return remote(
            packed.at[to],
            pool.at[pl.ds(owner * CAP, CAP)],
            block_send.at[to],
            block_recv.at[owner],
            dp,
            to,
            tp,
        )

    def send_blocks(off, carry):
        to = kv + off

        @pl.when(to < n_kv)
        def _():
            for slot in range(CAP):
                packed[to, slot] = own[requests_smem[to, 0, slot]]
            block_copy(kv, to).start()

        return carry

    lax.fori_loop(1, n_kv, send_blocks, 0)

    row_others = pair_all.at[pl.ds(0, (n_y - 1) * depth), :]
    drain(row_others, y_sem.at[1])
    drain(row_others, y_sem.at[3])

    above = lax.rem(z + 1, n_z) * n_y + y
    below = lax.rem(z + n_z - 1, n_z) * n_y + y
    bundle_depth = n_y * depth

    def bundle(ref, which):
        start = pl.multiple_of(lax.rem(which + n_z, n_z) * bundle_depth, bundle_depth)
        return ref.at[pl.ds(start, bundle_depth), my_cols]

    def ring(step, part, up):
        ref = (query_all, out_all)[part]
        piece = bundle(ref, z - step if up else z + step)
        at = (step * 2 + part) * 2 + (0 if up else 1)
        return remote(
            piece, piece, ring_send.at[at], ring_recv.at[at], dp, above if up else below, tp
        )

    half = n_z // 2
    started = []
    for step in range(half):
        now = []
        if step:
            for copy in started[-1]:
                copy.wait_recv()
        for part in range(2):
            for up in (True, False):
                if step == half - 1 and up != (part == 0):
                    continue
                now.append(ring(step, part, up))
        for copy in now:
            copy.start()
        started.append(now)
    for copy in started[-1]:
        copy.wait_recv()
    for group in started:
        for copy in group:
            copy.wait_send()

    right, left = lax.rem(dp + 1, n_dp), lax.rem(dp + n_dp - 1, n_dp)

    def columns(ref, which):
        start = pl.multiple_of(lax.rem(which + n_dp, n_dp) * quarter, quarter)
        return ref.at[:, pl.ds(start, quarter)]

    def across(at, ref, which, to):
        piece = columns(ref, which)
        return remote(piece, piece, x_send.at[at], x_recv.at[at], to, kv, tp)

    query_right, query_left = across(0, query_all, dp, right), across(1, query_all, dp, left)
    out_right, out_left = across(2, out_all, dp, right), across(3, out_all, dp, left)
    query_on = across(4, query_all, dp - 1, right)
    out_on = across(5, out_all, dp + 1, left)
    query_right.start()
    query_left.start()
    out_left.start()
    query_right.wait_recv()
    query_on.start()
    out_right.start()
    query_left.wait_recv()
    out_left.wait_recv()
    out_on.start()
    query_on.wait_recv()

    lane = lax.broadcasted_iota(jnp.int32, (tokens.shape[0], 2 * HEAD_WIDTH), 1)
    for d in range(n_dp):
        rows = jnp.dot(
            tokens[...],
            query_all[:, d * quarter : (d + 1) * quarter],
            preferred_element_type=jnp.float32,
        )
        rows = rows.astype(jnp.bfloat16).astype(jnp.float32) * HEAD_WIDTH ** (-0.5)
        turned = pltpu.roll(rows, HEAD_WIDTH, 1)
        for side, value in enumerate((rows, turned)):
            head = jnp.where(lane < HEAD_WIDTH, value, 0.0).astype(jnp.bfloat16)
            queries[:, 2 * d + side] = head.reshape(blocks, BLOCK_LENGTH, 2 * HEAD_WIDTH)

    def wait_blocks(owner, carry):
        @pl.when(owner < kv)
        def _():
            block_copy(owner, kv).wait_recv()

        return carry

    lax.fori_loop(0, n_kv, wait_blocks, 0)

    sel = placed_ref.shape[1]
    pair_rows = 2 * BLOCK_LENGTH
    row_at = lax.broadcasted_iota(jnp.int32, (pair_rows, 2 * HEAD_WIDTH), 0)
    lane_at = lax.broadcasted_iota(jnp.int32, (pair_rows, 2 * HEAD_WIDTH), 1)
    first_half = lane_at < BLOCK_LENGTH
    own_bias = jnp.where(lane_at <= lax.rem(row_at, BLOCK_LENGTH), 0.0, NEG)

    def attend(block, carry):
        shut = []
        for s in range(sel):
            at = placed_ref[block, s]
            gathered[s * BLOCK_LENGTH : (s + 1) * BLOCK_LENGTH, :] = pool[jnp.maximum(at, 0)]
            shut.append(jnp.where(at < 0, NEG, 0.0))
        bias = [jnp.where(first_half, own_bias, shut[1])]
        for s in range(2, sel, 2):
            bias.append(jnp.where(first_half, shut[s], shut[s + 1]))
        bias = jnp.concatenate(bias, axis=1)
        keys = gathered[...]
        outs = []
        for d in range(n_dp):
            query_pair = queries[block, 2 * d : 2 * d + 2].reshape(pair_rows, 2 * HEAD_WIDTH)
            scores = lax.dot_general(
                query_pair, keys, (((1,), (1,)), ((), ())), preferred_element_type=jnp.float32
            )
            scores = scores + bias
            expon = jnp.exp(scores - jnp.max(scores, axis=1, keepdims=True))
            total = jnp.sum(expon, axis=1, keepdims=True)
            probs = (expon * (1.0 / total)).astype(jnp.bfloat16)
            mixed = jnp.dot(probs, keys, preferred_element_type=jnp.float32)
            even = pltpu.roll(mixed[:BLOCK_LENGTH], HEAD_WIDTH, 1)
            odd = mixed[BLOCK_LENGTH:]
            outs.append(
                jnp.where(first_half[:BLOCK_LENGTH], even, odd).astype(jnp.bfloat16)
            )
        rows = pl.ds(pl.multiple_of(block * BLOCK_LENGTH, BLOCK_LENGTH), BLOCK_LENGTH)
        attended[rows, :] = jnp.concatenate(outs, axis=1)
        return carry

    lax.fori_loop(0, blocks, attend, 0)

    out_right.wait_recv()
    out_on.wait_recv()

    rows_out = part_mine.shape[0]

    def project(which):
        rows = attended[pl.ds(pl.multiple_of(which * rows_out, rows_out), rows_out), :]
        return lax.dot_general(
            rows, out_all[...], (((1,), (1,)), ((), ())), preferred_element_type=jnp.float32
        )

    part_send[...] = project(1 - tp).astype(jnp.bfloat16)
    swap = remote(part_send, part_recv, half_sem.at[0], half_sem.at[1], dp, kv, 1 - tp)
    swap.start()
    part_mine[...] = project(tp)
    swap.wait_recv()
    mixed = part_mine[...] + part_recv[...].astype(jnp.float32)
    scale = lax.rsqrt(jnp.mean(mixed * mixed, axis=1, keepdims=True) + 1e-06)
    result_ref[...] = (mixed * scale * gain_ref[...]).astype(jnp.bfloat16)

    drain(others, pair_sem.at[0])
    drain(requests_all.at[pl.ds(0, n_kv - 1)], request_sem.at[0])
    drain(row_others, y_sem.at[0])
    drain(row_others, y_sem.at[2])
    for copy in (query_right, query_left, out_right, out_left, query_on, out_on):
        copy.wait_send()

    def drain_blocks(to, carry):
        @pl.when(to > kv)
        def _():
            block_copy(kv, to).wait_send()

        return carry

    lax.fori_loop(0, n_kv, drain_blocks, 0)
    swap.wait_send()


def index_tables(chosen, device, n_kv, blocks):
    safe = jnp.maximum(chosen, 0)
    targets = jnp.arange(n_kv * blocks, dtype=jnp.int32)
    hit = (chosen.reshape(-1, 1) == targets[None, :]).astype(jnp.int32)
    wanted = jnp.max(hit, axis=0)
    grid = wanted.reshape(n_kv, blocks)
    place = jnp.arange(blocks, dtype=jnp.int32)
    below = (place[:, None] > place[None, :]).astype(jnp.int32)
    rank = jnp.sum(grid[:, None, :] * below[None], axis=2)
    slots = [jnp.max(jnp.where((grid > 0) & (rank == s), place[None], 0), axis=1) for s in range(CAP)]
    requests = jnp.pad(jnp.stack(slots, axis=1), ((0, 0), (0, 128 - CAP)))[:, None, :]
    flat = safe.reshape(-1, 1)
    same = (flat // blocks == targets[None, :] // blocks) & (targets[None, :] < flat)
    slot = jnp.minimum(jnp.sum(jnp.where(same, wanted[None, :], 0), axis=1), CAP - 1)
    slot = slot.reshape(chosen.shape)
    owner = safe // blocks
    placed = jnp.where(owner == device, n_kv * CAP + safe - owner * blocks, owner * CAP + slot)
    return requests, jnp.where(chosen < 0, -1, placed)


def per_device(dims, tokens, chosen, query_weight, key_matrix, value_matrix, out_weight, out_gain):
    n_dp, n_kv, n_y = dims
    rows, width = tokens.shape
    blocks = rows // BLOCK_LENGTH
    heads_width = query_weight.shape[1]
    requests, placed = index_tables(chosen, lax.axis_index("kv"), n_kv, blocks)
    pair = jnp.concatenate([key_matrix, value_matrix], axis=1)
    pair_width = pair.shape[1]
    half_rows = rows // 2
    vmem, dma = pltpu.VMEM, pltpu.SemaphoreType.DMA
    bf16, f32, i32 = jnp.bfloat16, jnp.float32, jnp.int32
    in_vmem = pl.BlockSpec(memory_space=pltpu.VMEM)
    return pl.pallas_call(
        functools.partial(fused_kernel, dims),
        out_shape=jax.ShapeDtypeStruct((half_rows, width), bf16),
        in_specs=[
            pl.BlockSpec(memory_space=pltpu.SMEM),
            in_vmem,
            pl.BlockSpec(memory_space=pl.ANY),
            in_vmem,
            in_vmem,
            in_vmem,
            in_vmem,
        ],
        out_specs=in_vmem,
        scratch_shapes=[
            vmem((rows, width), bf16),
            vmem((width, pair_width), bf16),
            vmem((n_kv, 1, 128), i32),
            pltpu.SMEM((n_kv, 1, 128), i32),
            vmem((width, heads_width), bf16),
            vmem((width, heads_width), bf16),
            vmem((blocks, BLOCK_LENGTH, pair_width), bf16),
            vmem((n_kv * CAP + blocks, BLOCK_LENGTH, pair_width), bf16),
            vmem((n_kv, CAP, BLOCK_LENGTH, pair_width), bf16),
            vmem((blocks, heads_width // HEAD_WIDTH, BLOCK_LENGTH, pair_width), bf16),
            vmem((chosen.shape[1] * BLOCK_LENGTH, pair_width), bf16),
            vmem((rows, heads_width), bf16),
            vmem((half_rows, width), f32),
            vmem((half_rows, width), bf16),
            vmem((half_rows, width), bf16),
            dma,
            dma,
            dma((2,)),
            dma((2,)),
            dma((4,)),
            dma((16,)),
            dma((16,)),
            dma((6,)),
            dma((6,)),
            dma((n_kv,)),
            dma((n_kv,)),
            dma((2,)),
        ],
        compiler_params=pltpu.CompilerParams(
            collective_id=0, has_side_effects=True, vmem_limit_bytes=60 * 1024 * 1024
        ),
        name="fused",
    )(placed, requests, tokens, pair, query_weight, out_weight.T, out_gain[None, :])


def solution(mesh):
    n_dp, n_kv = mesh.shape["dp"], mesh.shape["kv"]
    n_y = 8
    placed = (
        P(("dp", "kv"), None),
        P(("dp", "kv"), None),
        P("kv", "tp"),
        P("kv", "tp"),
        P("kv", "tp"),
        P("tp", "kv"),
        P(),
    )
    return jax.shard_map(
        functools.partial(per_device, (n_dp, n_kv, n_y)),
        mesh=mesh,
        in_specs=placed,
        out_specs=P(("dp", "kv", "tp"), None),
        check_vma=False,
    )
```

time: 247 us -> 163 us (0.66)
  Pallas kernels: 0 us -> 155 us
  waiting for transfers between devices: 90.8 us -> 0 us
  blocking collectives: 41.2 us -> 0 us
  matrix products: 35 us -> 0 us
  local copies, waits for them, and re-layouts: 30.1 us -> 4.09 us
  other arithmetic: 25.9 us -> 3.83 us
  between operations: 13.6 us -> 0.05 us
  starting transfers between devices: 8.8 us -> 0 us
    pallas_call x0 -> x1, Pallas kernels: none -> 155 us  [per_device(): pl.pallas_call(functools.partial(fused_kernel, dims), out_shape=jax.Shape...]
    all_gather x2 -> x0, waiting for transfers between devices: 57.5 us -> none  [the longest x1 57.5 us: side_by_side(): lax.all_gather(both, axis, axis=dim, tiled=True)]
    all_to_all x2 -> x0, blocking collectives: 41.2 us -> none  [the longest x1 27.8 us: per_device(): lax.all_to_all(requests, 'kv', split_axis=0, concat_axis=0, tiled=True)]
    dot_general x20 -> x0, matrix products: 35 us -> none  [the longest x8 14.4 us: attend_block(): jnp.einsum('qgd,skd->gqsk', query_block, block_keys, preferred_element_ty...]
    all_to_all x1 -> x0, waiting for transfers between devices: 32.7 us -> none  [per_device(): lax.all_to_all(fetched, 'kv', split_axis=0, concat_axis=0, tiled=True)]
    all_to_all x1 -> x0, starting transfers between devices: 8.57 us -> none  [per_device(): lax.all_to_all(fetched, 'kv', split_axis=0, concat_axis=0, tiled=True)]
    reduce_sum x11 -> x2, other arithmetic: 8.83 us -> 0.29 us  [the longest x1 0.19 us: index_tables(): jnp.sum(jnp.where(same, wanted[None, :], 0), axis=1)]
    squeeze x8 -> x0, local copies, waits for them, and re-layouts: 7.81 us -> none  [per_device(): attended = lax.map(attend_block, (grouped, picked, visible))]
  transfers between devices with their start and end apart: 3 -> 0, of which waited for: 2 -> 0; matrix products, arithmetic and copies ran while one was open for 30% -> 0% of each run, Pallas kernels for 0% -> 0%
where the time goes in v1:
time: 163 us
  Pallas kernels  155 us (95%)
  local copies, waits for them, and re-layouts  4.09 us (3%)
  other arithmetic  3.83 us (2%)
    pallas_call x1, Pallas kernels, per_device(): pl.pallas_call(functools.partial(fused_kernel, dims), out_shape=jax.Shape...  155 us

profile of v1, /device:TPU:1, one launch (start us, length us, event | category | flops | bytes accessed | tf_op | source)
XLA Modules:
  0.0 162.7 jit_solution(2348262920778756485)
XLA Ops:
  0.0 0.8 eq.46
  0.8 0.1 convert_reduce_fusion
  0.9 0.7 broadcast_maximum_fusion
  1.6 0.1 reshape.124
  1.7 0.2 select_reduce_fusion
  1.9 0.1 min.9
  2.0 1.3 select_select_fusion.placed_ref
  3.3 1.4 pad_maximum_fusion.pair_ref
  4.7 0.1 reshape.125
  4.7 0.1 copy.13
  4.8 0.1 multiply_reduce_fusion
  4.9 0.1 copy.15
  5.0 0.6 pad.4
  5.7 154.7 %fused.1 = bf16[256,2048]{1,0:T(8,128)(2,1)} custom-call(s32[8,16]{1,0:T(8,128)} %select_select_fusion.placed_ref, s32[64,1,128]{2,1,0:T(1,128)} %bitcast.5, bf16[512,2048]{1,0:T(8,128)(2,1)} %tokens_hbm.1, bf16[32,128]{1,0:T(8,128)(2,1)} %pad_maximum_fusion.pair_ref, bf16[32,512]{1,0:T(8,128)(2,1)} %query_ref.1, bf16[32,512]{1,0:T(8,128)(2,1)} %bitcast.6, ...), custom_call_target="tpu_custom_call" | custom-call | tf_op jit(solution)/shard_map/fused/pallas_call | solution.py:377
  160.4 2.3 %copy.17 = bf16[256,2048]{1,0:T(8,128)(2,1)} copy(bf16[256,2048]{1,0:T(8,128)(2,1)} %fused.1) | data formatting | bytes 2097152
  (6 shorter events, 0.1 us)

commit v2 on v1

--- a/solution.py
+++ b/solution.py
@@ -10,6 +10,7 @@
 HEAD_WIDTH = 64
 BLOCK_LENGTH = 64
 CAP = 2
+NEAR = 5
 NEG = -1e30
 MESH = pl.DeviceIdType.MESH
 
@@ -31,8 +32,14 @@
     query_all,
     out_all,
     own,
+    chain1,
+    chain2,
+    chain3,
+    chain4,
     pool,
     packed,
+    far_packed,
+    relayed,
     queries,
     gathered,
     attended,
@@ -48,8 +55,13 @@
     ring_recv,
     x_send,
     x_recv,
+    chain_send,
+    chain_recv,
     block_send,
     block_recv,
+    relay_send,
+    relay_recv,
+    onward_send,
     half_sem,
 ):
     n_dp, n_kv, n_y = dims
@@ -59,6 +71,9 @@
     depth = pair_ref.shape[0]
     blocks = own.shape[0]
     quarter = query_ref.shape[1] // n_dp
+    chains = (own, chain1, chain2, chain3, chain4)
+    near = len(chains)
+    n_far = n_z - near
 
     def remote(src, dst, send, recv, to_dp, to_kv, to_tp):
         return pltpu.make_async_remote_copy(
@@ -70,6 +85,9 @@
             device_id_type=MESH,
         )
 
+    def drain(ref, sem):
+        pltpu.make_async_copy(ref, ref, sem).wait()
+
     load_tokens = pltpu.make_async_copy(tokens_hbm, tokens, tok_sem)
     load_tokens.start()
 
@@ -95,152 +113,315 @@
 
     pl.semaphore_wait(barrier, n_kv - 1 + n_dp - 1 + 1)
 
+    def send_row(off, carry):
+        other = z * n_y + lax.rem(y + off, n_y)
+        for at, (src, dst) in enumerate(((query_ref, query_all), (out_ref, out_all))):
+            remote(
+                src.at[:, my_cols],
+                dst.at[my_rows, my_cols],
+                y_sem.at[2 * at],
+                y_sem.at[2 * at + 1],
+                dp,
+                other,
+                tp,
+            ).start()
+        return carry
+
+    lax.fori_loop(1, n_y, send_row, 0)
+
     def send_pair(off, carry):
         other = lax.rem(kv + off, n_kv)
         remote(
             pair_ref, pair_all.at[my_rows, :], pair_sem.at[0], pair_sem.at[1], dp, other, tp
         ).start()
+        return carry
+
+    lax.fori_loop(1, n_kv, send_pair, 0)
+
+    def ask(column, row, at):
         remote(
-            requests_ref.at[pl.ds(other, 1)],
-            requests_all.at[pl.ds(kv, 1)],
+            requests_ref.at[pl.ds(column, 1)],
+            requests_all.at[pl.ds(at, 1)],
             request_sem.at[0],
             request_sem.at[1],
             dp,
-            other,
+            row * n_y + column,
             tp,
         ).start()
-        return carry
-
-    lax.fori_loop(1, n_kv, send_pair, 0)
-
-    def send_row(off, carry):
-        other = z * n_y + lax.rem(y + off, n_y)
-        remote(
-            query_ref.at[:, my_cols],
-            query_all.at[my_rows, my_cols],
-            y_sem.at[0],
-            y_sem.at[1],
-            dp,
-            other,
-            tp,
-        ).start()
-        remote(
-            out_ref.at[:, my_cols],
-            out_all.at[my_rows, my_cols],
-            y_sem.at[2],
-            y_sem.at[3],
-            dp,
-            other,
-            tp,
-        ).start()
-        return carry
-
-    lax.fori_loop(1, n_y, send_row, 0)
-
-    def drain(ref, sem):
-        pltpu.make_async_copy(ref, ref, sem).wait()
+
+    def ask_row(off, carry):
+        ask(lax.rem(y + off, n_y), z, y)
+        return carry
+
+    def ask_far(column, carry):
+        for far in range(n_far):
+            ask(column, lax.rem(z + n_z - near - far, n_z), n_y * (1 + far) + y)
+        return carry
+
+    lax.fori_loop(1, n_y, ask_row, 0)
+    lax.fori_loop(0, n_y, ask_far, 0)
+    asked = requests_all.at[pl.ds(0, n_y * (1 + n_far) - 1)]
 
     others = pair_all.at[pl.ds(0, (n_kv - 1) * depth), :]
-    drain(others, pair_sem.at[1])
-    drain(requests_all.at[pl.ds(0, n_kv - 1)], request_sem.at[1])
+    row_others = pair_all.at[pl.ds(0, (n_y - 1) * depth), :]
+
+    above = lax.rem(z + 1, n_z) * n_y + y
+    below = lax.rem(z + n_z - 1, n_z) * n_y + y
+    right, left = lax.rem(dp + 1, n_dp), lax.rem(dp + n_dp - 1, n_dp)
+    bundle_depth = n_y * depth
+    downs = 2
+    ups = n_z - 1 - downs
+
+    def bundle(ref, delta, which):
+        start = pl.multiple_of(lax.rem(z + n_z + delta, n_z) * bundle_depth, bundle_depth)
+        cols = pl.multiple_of(lax.rem(dp + n_dp + which, n_dp) * quarter, quarter)
+        return ref.at[pl.ds(start, bundle_depth), pl.ds(cols, quarter)]
+
+    def ring(step, up):
+        copies = []
+        for part, ref in enumerate((query_all, out_all)):
+            piece = bundle(ref, 1 - step if up else step - 1, 0)
+            at = 2 * (step - 1 if up else ups + step - 1) + part
+            copies.append(
+                remote(
+                    piece, piece, ring_send.at[at], ring_recv.at[at], dp, above if up else below, tp
+                )
+            )
+        return copies
+
+    def across(delta, kind):
+        ref = out_all if kind in (2, 3, 5) else query_all
+        which = {4: -1, 5: 1}.get(kind, 0)
+        piece = bundle(ref, delta, which)
+        at = lax.rem(z + n_z + delta, n_z) * 6 + kind
+        to = right if kind in (0, 2, 4) else left
+        return remote(piece, piece, x_send.at[at], x_recv.at[at], to, kv, tp)
+
+    def cross(delta):
+        for kind in range(4):
+            across(delta, kind).start()
+
+    def cross_on(delta):
+        across(delta, 0).wait_recv()
+        across(delta, 4).start()
+        across(delta, 3).wait_recv()
+        across(delta, 5).start()
+
+    def start(copies):
+        for copy in copies:
+            copy.start()
+
+    def arrive(copies):
+        for copy in copies:
+            copy.wait_recv()
+
+    drain(row_others, y_sem.at[1])
+    drain(row_others, y_sem.at[3])
+    start(ring(1, True))
+    start(ring(1, False))
+    cross(0)
+
+    drain(asked, request_sem.at[1])
     to_smem = pltpu.make_async_copy(requests_all, requests_smem, smem_sem)
     to_smem.start()
     load_tokens.wait()
+    drain(others, pair_sem.at[1])
     pairs = jnp.dot(tokens[...], pair_all[...], preferred_element_type=jnp.float32)
     pairs = pairs.astype(jnp.bfloat16).reshape(own.shape)
     own[...] = pairs
     pool[pl.ds(n_kv * CAP, blocks)] = pairs
     to_smem.wait()
 
-    def block_copy(owner, to):
+    def climb(step):
         return remote(
-            packed.at[to],
-            pool.at[pl.ds(owner * CAP, CAP)],
-            block_send.at[to],
+            chains[step - 1],
+            chains[step],
+            chain_send.at[step - 1],
+            chain_recv.at[step - 1],
+            dp,
+            above,
+            tp,
+        )
+
+    def climb_on(step):
+        @pl.when((z + 1 < n_z) & (z >= step - 1))
+        def _():
+            climb(step).start()
+
+    def slots(owner):
+        return pool.at[pl.ds(owner * CAP, CAP)]
+
+    def far_copy(far, column):
+        return remote(
+            far_packed.at[far, column],
+            relayed.at[far, y],
+            relay_send.at[far * n_y + column],
+            relay_recv.at[far * n_y + y],
+            dp,
+            z * n_y + column,
+            tp,
+        )
+
+    def far_own(far):
+        return remote(
+            far_packed.at[far, y],
+            slots(kv),
+            relay_send.at[far * n_y + y],
+            block_recv.at[kv],
+            dp,
+            (z + near + far) * n_y + y,
+            tp,
+        )
+
+    def onward(far, column):
+        owner = z * n_y + column
+        return remote(
+            relayed.at[far, column],
+            slots(owner),
+            onward_send.at[far * n_y + column],
             block_recv.at[owner],
             dp,
-            to,
+            (z + near + far) * n_y + y,
             tp,
         )
 
-    def send_blocks(off, carry):
-        to = kv + off
-
-        @pl.when(to < n_kv)
+    def send_far(far):
+        def one(off, carry):
+            column = lax.rem(y + off, n_y)
+            for slot in range(CAP):
+                at = requests_smem[n_y * (1 + far) + column, 0, CAP * (near + far) + slot]
+                far_packed[far, column, slot] = own[at]
+
+            @pl.when(off > 0)
+            def _():
+                far_copy(far, column).start()
+
+            @pl.when(off == 0)
+            def _():
+                far_own(far).start()
+
+            return carry
+
+        @pl.when(z + near + far < n_z)
         def _():
-            for slot in range(CAP):
-                packed[to, slot] = own[requests_smem[to, 0, slot]]
-            block_copy(kv, to).start()
-
-        return carry
-
-    lax.fori_loop(1, n_kv, send_blocks, 0)
-
-    row_others = pair_all.at[pl.ds(0, (n_y - 1) * depth), :]
-    drain(row_others, y_sem.at[1])
-    drain(row_others, y_sem.at[3])
-
-    above = lax.rem(z + 1, n_z) * n_y + y
-    below = lax.rem(z + n_z - 1, n_z) * n_y + y
-    bundle_depth = n_y * depth
-
-    def bundle(ref, which):
-        start = pl.multiple_of(lax.rem(which + n_z, n_z) * bundle_depth, bundle_depth)
-        return ref.at[pl.ds(start, bundle_depth), my_cols]
-
-    def ring(step, part, up):
-        ref = (query_all, out_all)[part]
-        piece = bundle(ref, z - step if up else z + step)
-        at = (step * 2 + part) * 2 + (0 if up else 1)
+            lax.fori_loop(0, n_y, one, 0)
+
+    def pass_far(far):
+        def one(off, carry):
+            column = lax.rem(y + off, n_y)
+            relay = remote(
+                far_packed.at[far, y],
+                relayed.at[far, column],
+                relay_send.at[far * n_y + y],
+                relay_recv.at[far * n_y + column],
+                dp,
+                kv,
+                tp,
+            )
+            relay.wait_recv()
+            onward(far, column).start()
+            return carry
+
+        @pl.when(z + near + far < n_z)
+        def _():
+            lax.fori_loop(1, n_y, one, 0)
+
+    def near_copy(step, column):
+        owner = (z - step) * n_y + y
         return remote(
-            piece, piece, ring_send.at[at], ring_recv.at[at], dp, above if up else below, tp
-        )
-
-    half = n_z // 2
-    started = []
-    for step in range(half):
-        now = []
-        if step:
-            for copy in started[-1]:
-                copy.wait_recv()
-        for part in range(2):
-            for up in (True, False):
-                if step == half - 1 and up != (part == 0):
-                    continue
-                now.append(ring(step, part, up))
-        for copy in now:
-            copy.start()
-        started.append(now)
-    for copy in started[-1]:
-        copy.wait_recv()
-    for group in started:
-        for copy in group:
-            copy.wait_send()
-
-    right, left = lax.rem(dp + 1, n_dp), lax.rem(dp + n_dp - 1, n_dp)
-
-    def columns(ref, which):
-        start = pl.multiple_of(lax.rem(which + n_dp, n_dp) * quarter, quarter)
-        return ref.at[:, pl.ds(start, quarter)]
-
-    def across(at, ref, which, to):
-        piece = columns(ref, which)
-        return remote(piece, piece, x_send.at[at], x_recv.at[at], to, kv, tp)
-
-    query_right, query_left = across(0, query_all, dp, right), across(1, query_all, dp, left)
-    out_right, out_left = across(2, out_all, dp, right), across(3, out_all, dp, left)
-    query_on = across(4, query_all, dp - 1, right)
-    out_on = across(5, out_all, dp + 1, left)
-    query_right.start()
-    query_left.start()
-    out_left.start()
-    query_right.wait_recv()
-    query_on.start()
-    out_right.start()
-    query_left.wait_recv()
-    out_left.wait_recv()
-    out_on.start()
-    query_on.wait_recv()
+            packed.at[step, column],
+            slots(owner),
+            block_send.at[step * n_y + column],
+            block_recv.at[owner],
+            dp,
+            z * n_y + column,
+            tp,
+        )
+
+    def share(step):
+        def one(off, carry):
+            column = lax.rem(y + off, n_y)
+
+            @pl.when((column > y) | (step > 0))
+            def _():
+                for slot in range(CAP):
+                    at = requests_smem[column, 0, CAP * step + slot]
+                    packed[step, column, slot] = chains[step][at]
+                near_copy(step, column).start()
+
+            return carry
+
+        lax.fori_loop(1, n_y, one, 0)
+
+    def take_chain(step):
+        @pl.when(z >= step)
+        def _():
+            climb(step).wait_recv()
+
+        if step + 1 < near:
+            climb_on(step + 1)
+
+        @pl.when(z >= step)
+        def _():
+            pool[pl.ds(n_kv * CAP + step * blocks, blocks)] = chains[step][...]
+            share(step)
+
+    climb_on(1)
+    for far in reversed(range(n_far)):
+        send_far(far)
+    share(0)
+
+    arrive(ring(1, True))
+    arrive(ring(1, False))
+    start(ring(2, True))
+    start(ring(2, False))
+    cross(-1)
+    cross(1)
+
+    pass_far(2)
+    take_chain(1)
+    cross_on(0)
+
+    arrive(ring(2, True))
+    arrive(ring(2, False))
+    start(ring(3, True))
+    cross(-2)
+    cross(2)
+
+    pass_far(1)
+    take_chain(2)
+    cross_on(-1)
+    cross_on(1)
+
+    arrive(ring(3, True))
+    start(ring(4, True))
+    cross(-3)
+
+    pass_far(0)
+    take_chain(3)
+    cross_on(-2)
+    cross_on(2)
+
+    arrive(ring(4, True))
+    start(ring(5, True))
+    cross(-4)
+
+    take_chain(4)
+    cross_on(-3)
+    arrive(ring(5, True))
+    cross(-5)
+    cross_on(-4)
+    cross_on(-5)
+
+    def wait_across(kinds):
+        def one(at, carry):
+            for kind in kinds:
+                across(at - z, kind).wait_recv()
+            return carry
+
+        lax.fori_loop(0, n_z, one, 0)
+
+    wait_across((1, 4))
 
     lane = lax.broadcasted_iota(jnp.int32, (tokens.shape[0], 2 * HEAD_WIDTH), 1)
     for d in range(n_dp):
@@ -256,9 +437,15 @@
             queries[:, 2 * d + side] = head.reshape(blocks, BLOCK_LENGTH, 2 * HEAD_WIDTH)
 
     def wait_blocks(owner, carry):
-        @pl.when(owner < kv)
+        steps = z - owner // n_y
+        mate = lax.rem(owner, n_y)
+        expected = (owner < kv) & ((steps == 0) | (steps >= near) | (mate != y))
+
+        @pl.when(expected)
         def _():
-            block_copy(owner, kv).wait_recv()
+            remote(
+                packed.at[0, 0], slots(owner), block_send.at[0], block_recv.at[owner], dp, kv, tp
+            ).wait_recv()
 
         return carry
 
@@ -304,8 +491,7 @@
 
     lax.fori_loop(0, blocks, attend, 0)
 
-    out_right.wait_recv()
-    out_on.wait_recv()
+    wait_across((2, 5))
 
     rows_out = part_mine.shape[0]
 
@@ -325,24 +511,63 @@
     result_ref[...] = (mixed * scale * gain_ref[...]).astype(jnp.bfloat16)
 
     drain(others, pair_sem.at[0])
-    drain(requests_all.at[pl.ds(0, n_kv - 1)], request_sem.at[0])
+    drain(asked, request_sem.at[0])
     drain(row_others, y_sem.at[0])
     drain(row_others, y_sem.at[2])
-    for copy in (query_right, query_left, out_right, out_left, query_on, out_on):
-        copy.wait_send()
-
-    def drain_blocks(to, carry):
-        @pl.when(to > kv)
-        def _():
-            block_copy(kv, to).wait_send()
-
-        return carry
-
-    lax.fori_loop(0, n_kv, drain_blocks, 0)
+    for step in range(1, ups + 1):
+        for copy in ring(step, True):
+            copy.wait_send()
+    for step in range(1, downs + 1):
+        for copy in ring(step, False):
+            copy.wait_send()
+
+    def drain_across(at, carry):
+        for kind in range(6):
+            across(at - z, kind).wait_send()
+        return carry
+
+    lax.fori_loop(0, n_z, drain_across, 0)
+
+    for step in range(near):
+        if step + 1 < near:
+
+            @pl.when((z + 1 < n_z) & (z >= step))
+            def _(step=step):
+                climb(step + 1).wait_send()
+
+        def drain_near(off, carry, step=step):
+            column = lax.rem(y + off, n_y)
+
+            @pl.when((z >= step) & ((column > y) | (step > 0)))
+            def _():
+                near_copy(step, column).wait_send()
+
+            return carry
+
+        lax.fori_loop(1, n_y, drain_near, 0)
+
+    for far in range(n_far):
+
+        def drain_far(off, carry, far=far):
+            column = lax.rem(y + off, n_y)
+            far_copy(far, column).wait_send()
+
+            @pl.when(off > 0)
+            def _():
+                onward(far, column).wait_send()
+
+            return carry
+
+        @pl.when(z + near + far < n_z)
+        def _(drain_far=drain_far):
+            lax.fori_loop(0, n_y, drain_far, 0)
+
     swap.wait_send()
 
 
-def index_tables(chosen, device, n_kv, blocks):
+def index_tables(chosen, device, n_kv, n_y, blocks):
+    n_z = n_kv // n_y
+    z, y = device // n_y, device % n_y
     safe = jnp.maximum(chosen, 0)
     targets = jnp.arange(n_kv * blocks, dtype=jnp.int32)
     hit = (chosen.reshape(-1, 1) == targets[None, :]).astype(jnp.int32)
@@ -352,13 +577,19 @@
     below = (place[:, None] > place[None, :]).astype(jnp.int32)
     rank = jnp.sum(grid[:, None, :] * below[None], axis=2)
     slots = [jnp.max(jnp.where((grid > 0) & (rank == s), place[None], 0), axis=1) for s in range(CAP)]
-    requests = jnp.pad(jnp.stack(slots, axis=1), ((0, 0), (0, 128 - CAP)))[:, None, :]
+    table = jnp.stack(slots, axis=1).reshape(n_z, n_y, CAP)
+    table = jnp.take(table, (z - jnp.arange(n_z)) % n_z, axis=0)
+    table = table.transpose(1, 0, 2).reshape(n_y, n_z * CAP)
+    requests = jnp.pad(table, ((0, 0), (0, 128 - n_z * CAP)))[:, None, :]
     flat = safe.reshape(-1, 1)
     same = (flat // blocks == targets[None, :] // blocks) & (targets[None, :] < flat)
     slot = jnp.minimum(jnp.sum(jnp.where(same, wanted[None, :], 0), axis=1), CAP - 1)
     slot = slot.reshape(chosen.shape)
     owner = safe // blocks
-    placed = jnp.where(owner == device, n_kv * CAP + safe - owner * blocks, owner * CAP + slot)
+    steps = z - owner // n_y
+    whole = (owner % n_y == y) & (steps >= 0) & (steps < NEAR)
+    inside = n_kv * CAP + steps * blocks + safe - owner * blocks
+    placed = jnp.where(whole, inside, owner * CAP + slot)
     return requests, jnp.where(chosen < 0, -1, placed)
 
 
@@ -367,10 +598,12 @@
     rows, width = tokens.shape
     blocks = rows // BLOCK_LENGTH
     heads_width = query_weight.shape[1]
-    requests, placed = index_tables(chosen, lax.axis_index("kv"), n_kv, blocks)
+    requests, placed = index_tables(chosen, lax.axis_index("kv"), n_kv, n_y, blocks)
     pair = jnp.concatenate([key_matrix, value_matrix], axis=1)
     pair_width = pair.shape[1]
     half_rows = rows // 2
+    n_z = n_kv // n_y
+    far = n_z - NEAR
     vmem, dma = pltpu.VMEM, pltpu.SemaphoreType.DMA
     bf16, f32, i32 = jnp.bfloat16, jnp.float32, jnp.int32
     in_vmem = pl.BlockSpec(memory_space=pltpu.VMEM)
@@ -390,13 +623,15 @@
         scratch_shapes=[
             vmem((rows, width), bf16),
             vmem((width, pair_width), bf16),
-            vmem((n_kv, 1, 128), i32),
-            pltpu.SMEM((n_kv, 1, 128), i32),
+            vmem((n_y * (1 + far), 1, 128), i32),
+            pltpu.SMEM((n_y * (1 + far), 1, 128), i32),
             vmem((width, heads_width), bf16),
             vmem((width, heads_width), bf16),
-            vmem((blocks, BLOCK_LENGTH, pair_width), bf16),
-            vmem((n_kv * CAP + blocks, BLOCK_LENGTH, pair_width), bf16),
-            vmem((n_kv, CAP, BLOCK_LENGTH, pair_width), bf16),
+            *[vmem((blocks, BLOCK_LENGTH, pair_width), bf16)] * NEAR,
+            vmem((n_kv * CAP + NEAR * blocks, BLOCK_LENGTH, pair_width), bf16),
+            vmem((NEAR, n_y, CAP, BLOCK_LENGTH, pair_width), bf16),
+            vmem((far, n_y, CAP, BLOCK_LENGTH, pair_width), bf16),
+            vmem((far, n_y, CAP, BLOCK_LENGTH, pair_width), bf16),
             vmem((blocks, heads_width // HEAD_WIDTH, BLOCK_LENGTH, pair_width), bf16),
             vmem((chosen.shape[1] * BLOCK_LENGTH, pair_width), bf16),
             vmem((rows, heads_width), bf16),
@@ -408,12 +643,17 @@
             dma((2,)),
             dma((2,)),
             dma((4,)),
-            dma((16,)),
-            dma((16,)),
-            dma((6,)),
-            dma((6,)),
+            dma((2 * (n_z - 1),)),
+            dma((2 * (n_z - 1),)),
+            dma((6 * n_z,)),
+            dma((6 * n_z,)),
+            dma((NEAR - 1,)),
+            dma((NEAR - 1,)),
+            dma((NEAR * n_y,)),
             dma((n_kv,)),
-            dma((n_kv,)),
+            dma((far * n_y,)),
+            dma((far * n_y,)),
+            dma((far * n_y,)),
             dma((2,)),
         ],
         compiler_params=pltpu.CompilerParams(

time: 163 us -> 112 us (0.69)
  Pallas kernels: 155 us -> 103 us
    pallas_call x1, Pallas kernels: 155 us -> 103 us  [per_device(): pl.pallas_call(functools.partial(fused_kernel, dims), out_shape=jax.Shape...]
where the time goes in v2:
time: 112 us
  Pallas kernels  103 us (92%)
  local copies, waits for them, and re-layouts  4.78 us (4%)
  other arithmetic  3.96 us (4%)
    pallas_call x1, Pallas kernels, per_device(): pl.pallas_call(functools.partial(fused_kernel, dims), out_shape=jax.Shape...  103 us
    unnamed x1, local copies, waits for them, and re-layouts  2.3 us

profile of v2, /device:TPU:1, one launch (start us, length us, event | category | flops | bytes accessed | tf_op | source)
XLA Modules:
  0.0 111.5 jit_solution(14793324997472139584)
XLA Ops:
  0.0 0.8 eq.52
  0.8 0.1 convert_reduce_fusion
  0.9 0.7 broadcast_maximum_fusion
  1.6 0.1 reshape.186
  1.7 0.2 select_reduce_fusion
  1.9 0.1 min.9
  2.0 1.3 %select_select_fusion.placed_ref = s32[8,16]{1,0:T(8,128)} fusion(s32[8,16]{1,0:T(8,128)S(1)} %min.9, s32[8,16]{1,0:T(8,128)} %param.8, s32[]{:T(128)S(6)} %select_n.107, s32[]{:T(128)S(6)} %select_n.106), kind=kLoop, calls=%fused_computation.22 | loop fusion | flops 5632 | bytes 1544 | tf_op jit(solution)/shard_map/jit(_where)/select_n | solution.py:593
  3.3 1.4 %pad_maximum_fusion.pair_ref = bf16[32,128]{1,0:T(8,128)(2,1)} fusion(bf16[32,64]{1,0:T(8,128)(2,1)} %param.11, bf16[32,64]{1,0:T(8,128)(2,1)} %param.10), kind=kLoop, calls=%fused_computation.8 | loop fusion | flops 16384 | bytes 16384 | tf_op jit(solution)/shard_map/concatenate | solution.py:602
  4.7 0.1 reshape.187
  4.8 0.1 copy.13
  4.9 0.1 multiply_reduce_fusion
  5.0 0.1 stack.9
  5.1 0.1 stack.10
  5.2 0.6 gather_fusion
  5.7 0.1 broadcast_select_fusion
  5.8 0.1 copy.17
  5.9 0.6 pad.4
  6.5 102.7 %fused.1 = bf16[256,2048]{1,0:T(8,128)(2,1)} custom-call(s32[8,16]{1,0:T(8,128)} %select_select_fusion.placed_ref, s32[8,1,128]{2,1,0:T(1,128)} %bitcast.12, bf16[512,2048]{1,0:T(8,128)(2,1)} %tokens_hbm.1, bf16[32,128]{1,0:T(8,128)(2,1)} %pad_maximum_fusion.pair_ref, bf16[32,512]{1,0:T(8,128)(2,1)} %query_ref.1, bf16[32,512]{1,0:T(8,128)(2,1)} %bitcast.10, ...), custom_call_target="tpu_custom_call" | custom-call | tf_op jit(solution)/shard_map/fused/pallas_call | solution.py:610
  109.2 2.3 %copy.19 = bf16[256,2048]{1,0:T(8,128)(2,1)} copy(bf16[256,2048]{1,0:T(8,128)(2,1)} %fused.1) | data formatting | bytes 2097152
  (9 shorter events, 0.1 us)

commit v3 on v2

--- a/solution.py
+++ b/solution.py
@@ -17,14 +17,17 @@
 
 def fused_kernel(
     dims,
+    chosen_ref,
+    chosen_rows,
+    tokens_hbm,
+    key_ref,
+    value_ref,
+    query_ref,
+    out_ref,
+    result_ref,
+    placed_vmem,
     placed_ref,
     requests_ref,
-    tokens_hbm,
-    pair_ref,
-    query_ref,
-    out_ref,
-    gain_ref,
-    result_ref,
     tokens,
     pair_all,
     requests_all,
@@ -47,6 +50,7 @@
     part_send,
     part_recv,
     tok_sem,
+    place_sem,
     smem_sem,
     pair_sem,
     request_sem,
@@ -68,7 +72,7 @@
     n_z = n_kv // n_y
     dp, kv, tp = lax.axis_index("dp"), lax.axis_index("kv"), lax.axis_index("tp")
     z, y = kv // n_y, lax.rem(kv, n_y)
-    depth = pair_ref.shape[0]
+    depth = key_ref.shape[0]
     blocks = own.shape[0]
     quarter = query_ref.shape[1] // n_dp
     chains = (own, chain1, chain2, chain3, chain4)
@@ -107,17 +111,53 @@
 
     my_rows = pl.ds(pl.multiple_of(kv * depth, depth), depth)
     my_cols = pl.ds(pl.multiple_of(dp * quarter, quarter), quarter)
-    pair_all[my_rows, :] = pair_ref[...]
+    wide = jnp.float32
+    pair = jnp.concatenate([key_ref[...].astype(wide), value_ref[...].astype(wide)], axis=1)
+    pair_all[my_rows, :] = pair.astype(jnp.bfloat16)
     query_all[my_rows, my_cols] = query_ref[:, my_cols]
     out_all[my_rows, my_cols] = out_ref[:, my_cols]
 
+    sel = chosen_ref.shape[1]
+    table_lane = lax.broadcasted_iota(jnp.int32, (n_y, 128), 1)
+    table_owner = lax.rem(z + n_z - lax.rem(table_lane // CAP, n_z), n_z) * n_y
+    table_owner = table_owner + lax.broadcasted_iota(jnp.int32, (n_y, 128), 0)
+    table_last = lax.rem(table_lane, CAP) > 0
+    rows_at = chosen_rows[...]
+    rows_owner = jnp.right_shift(rows_at, 3)
+
+    def tabulate(at, carry):
+        first, last, later = carry
+        for s in range(sel):
+            block = chosen_ref[at, s]
+            owner = jnp.right_shift(block, 3)
+            inner = jnp.bitwise_and(block, blocks - 1)
+            mine = table_owner == owner
+            first = jnp.where(mine, jnp.minimum(first, inner), first)
+            last = jnp.where(mine, jnp.maximum(last, inner), last)
+            later = jnp.where((rows_owner == owner) & (rows_at > block), 1, later)
+        return first, last, later
+
+    zeros = jnp.zeros((n_y, 128), jnp.int32)
+    first, last, later = lax.fori_loop(
+        0, blocks, tabulate, (zeros + (blocks - 1), zeros, jnp.zeros(rows_at.shape, jnp.int32))
+    )
+    requests_ref[...] = jnp.where(table_last, last, first).reshape(requests_ref.shape)
+    steps_up = z - jnp.right_shift(rows_owner, 3)
+    whole = (jnp.bitwise_and(rows_owner, n_y - 1) == y) & (steps_up < near)
+    inside = n_kv * CAP + steps_up * blocks + jnp.bitwise_and(rows_at, blocks - 1)
+    placed = jnp.where(whole, inside, rows_owner * CAP + later)
+    placed_vmem[...] = jnp.zeros_like(placed_vmem)
+    placed_vmem[:, :sel] = jnp.where(rows_at < 0, -1, placed)
+    to_placed = pltpu.make_async_copy(placed_vmem, placed_ref, place_sem)
+    to_placed.start()
+
     pl.semaphore_wait(barrier, n_kv - 1 + n_dp - 1 + 1)
 
     def send_row(off, carry):
         other = z * n_y + lax.rem(y + off, n_y)
-        for at, (src, dst) in enumerate(((query_ref, query_all), (out_ref, out_all))):
+        for at, dst in enumerate((query_all, out_all)):
             remote(
-                src.at[:, my_cols],
+                dst.at[my_rows, my_cols],
                 dst.at[my_rows, my_cols],
                 y_sem.at[2 * at],
                 y_sem.at[2 * at + 1],
@@ -131,9 +171,8 @@
 
     def send_pair(off, carry):
         other = lax.rem(kv + off, n_kv)
-        remote(
-            pair_ref, pair_all.at[my_rows, :], pair_sem.at[0], pair_sem.at[1], dp, other, tp
-        ).start()
+        mine = pair_all.at[my_rows, :]
+        remote(mine, mine, pair_sem.at[0], pair_sem.at[1], dp, other, tp).start()
         return carry
 
     lax.fori_loop(1, n_kv, send_pair, 0)
@@ -220,6 +259,12 @@
     start(ring(1, True))
     start(ring(1, False))
     cross(0)
+    arrive(ring(1, True))
+    arrive(ring(1, False))
+    start(ring(2, True))
+    start(ring(2, False))
+    cross(-1)
+    cross(1)
 
     drain(asked, request_sem.at[1])
     to_smem = pltpu.make_async_copy(requests_all, requests_smem, smem_sem)
@@ -370,16 +415,6 @@
     for far in reversed(range(n_far)):
         send_far(far)
     share(0)
-
-    arrive(ring(1, True))
-    arrive(ring(1, False))
-    start(ring(2, True))
-    start(ring(2, False))
-    cross(-1)
-    cross(1)
-
-    pass_far(2)
-    take_chain(1)
     cross_on(0)
 
     arrive(ring(2, True))
@@ -387,29 +422,29 @@
     start(ring(3, True))
     cross(-2)
     cross(2)
-
-    pass_far(1)
-    take_chain(2)
+    pass_far(2)
+    take_chain(1)
     cross_on(-1)
     cross_on(1)
 
     arrive(ring(3, True))
     start(ring(4, True))
     cross(-3)
-
-    pass_far(0)
-    take_chain(3)
+    pass_far(1)
+    take_chain(2)
     cross_on(-2)
-    cross_on(2)
 
     arrive(ring(4, True))
     start(ring(5, True))
     cross(-4)
-
-    take_chain(4)
+    pass_far(0)
+    take_chain(3)
+    cross_on(2)
     cross_on(-3)
+
     arrive(ring(5, True))
     cross(-5)
+    take_chain(4)
     cross_on(-4)
     cross_on(-5)
 
@@ -436,6 +471,51 @@
             head = jnp.where(lane < HEAD_WIDTH, value, 0.0).astype(jnp.bfloat16)
             queries[:, 2 * d + side] = head.reshape(blocks, BLOCK_LENGTH, 2 * HEAD_WIDTH)
 
+    drain(others, pair_sem.at[0])
+    drain(asked, request_sem.at[0])
+    drain(row_others, y_sem.at[0])
+    drain(row_others, y_sem.at[2])
+    for step in range(1, ups + 1):
+        for copy in ring(step, True):
+            copy.wait_send()
+    for step in range(1, downs + 1):
+        for copy in ring(step, False):
+            copy.wait_send()
+
+    for step in range(near):
+        if step + 1 < near:
+
+            @pl.when((z + 1 < n_z) & (z >= step))
+            def _(step=step):
+                climb(step + 1).wait_send()
+
+        def drain_near(off, carry, step=step):
+            column = lax.rem(y + off, n_y)
+
+            @pl.when((z >= step) & ((column > y) | (step > 0)))
+            def _():
+                near_copy(step, column).wait_send()
+
+            return carry
+
+        lax.fori_loop(1, n_y, drain_near, 0)
+
+    for far in range(n_far):
+
+        def drain_far(off, carry, far=far):
+            column = lax.rem(y + off, n_y)
+            far_copy(far, column).wait_send()
+
+            @pl.when(off > 0)
+            def _():
+                onward(far, column).wait_send()
+
+            return carry
+
+        @pl.when(z + near + far < n_z)
+        def _(drain_far=drain_far):
+            lax.fori_loop(0, n_y, drain_far, 0)
+
     def wait_blocks(owner, carry):
         steps = z - owner // n_y
         mate = lax.rem(owner, n_y)
@@ -450,8 +530,8 @@
         return carry
 
     lax.fori_loop(0, n_kv, wait_blocks, 0)
-
-    sel = placed_ref.shape[1]
+    to_placed.wait()
+
     pair_rows = 2 * BLOCK_LENGTH
     row_at = lax.broadcasted_iota(jnp.int32, (pair_rows, 2 * HEAD_WIDTH), 0)
     lane_at = lax.broadcasted_iota(jnp.int32, (pair_rows, 2 * HEAD_WIDTH), 1)
@@ -478,8 +558,8 @@
             scores = scores + bias
             expon = jnp.exp(scores - jnp.max(scores, axis=1, keepdims=True))
             total = jnp.sum(expon, axis=1, keepdims=True)
-            probs = (expon * (1.0 / total)).astype(jnp.bfloat16)
-            mixed = jnp.dot(probs, keys, preferred_element_type=jnp.float32)
+            probs = expon.astype(jnp.bfloat16)
+            mixed = jnp.dot(probs, keys, preferred_element_type=jnp.float32) * (1.0 / total)
             even = pltpu.roll(mixed[:BLOCK_LENGTH], HEAD_WIDTH, 1)
             odd = mixed[BLOCK_LENGTH:]
             outs.append(
@@ -493,6 +573,13 @@
 
     wait_across((2, 5))
 
+    def drain_across(at, carry):
+        for kind in range(6):
+            across(at - z, kind).wait_send()
+        return carry
+
+    lax.fori_loop(0, n_z, drain_across, 0)
+
     rows_out = part_mine.shape[0]
 
     def project(which):
@@ -508,89 +595,9 @@
     swap.wait_recv()
     mixed = part_mine[...] + part_recv[...].astype(jnp.float32)
     scale = lax.rsqrt(jnp.mean(mixed * mixed, axis=1, keepdims=True) + 1e-06)
-    result_ref[...] = (mixed * scale * gain_ref[...]).astype(jnp.bfloat16)
-
-    drain(others, pair_sem.at[0])
-    drain(asked, request_sem.at[0])
-    drain(row_others, y_sem.at[0])
-    drain(row_others, y_sem.at[2])
-    for step in range(1, ups + 1):
-        for copy in ring(step, True):
-            copy.wait_send()
-    for step in range(1, downs + 1):
-        for copy in ring(step, False):
-            copy.wait_send()
-
-    def drain_across(at, carry):
-        for kind in range(6):
-            across(at - z, kind).wait_send()
-        return carry
-
-    lax.fori_loop(0, n_z, drain_across, 0)
-
-    for step in range(near):
-        if step + 1 < near:
-
-            @pl.when((z + 1 < n_z) & (z >= step))
-            def _(step=step):
-                climb(step + 1).wait_send()
-
-        def drain_near(off, carry, step=step):
-            column = lax.rem(y + off, n_y)
-
-            @pl.when((z >= step) & ((column > y) | (step > 0)))
-            def _():
-                near_copy(step, column).wait_send()
-
-            return carry
-
-        lax.fori_loop(1, n_y, drain_near, 0)
-
-    for far in range(n_far):
-
-        def drain_far(off, carry, far=far):
-            column = lax.rem(y + off, n_y)
-            far_copy(far, column).wait_send()
-
-            @pl.when(off > 0)
-            def _():
-                onward(far, column).wait_send()
-
-            return carry
-
-        @pl.when(z + near + far < n_z)
-        def _(drain_far=drain_far):
-            lax.fori_loop(0, n_y, drain_far, 0)
+    result_ref[...] = mixed * scale
 
     swap.wait_send()
-
-
-def index_tables(chosen, device, n_kv, n_y, blocks):
-    n_z = n_kv // n_y
-    z, y = device // n_y, device % n_y
-    safe = jnp.maximum(chosen, 0)
-    targets = jnp.arange(n_kv * blocks, dtype=jnp.int32)
-    hit = (chosen.reshape(-1, 1) == targets[None, :]).astype(jnp.int32)
-    wanted = jnp.max(hit, axis=0)
-    grid = wanted.reshape(n_kv, blocks)
-    place = jnp.arange(blocks, dtype=jnp.int32)
-    below = (place[:, None] > place[None, :]).astype(jnp.int32)
-    rank = jnp.sum(grid[:, None, :] * below[None], axis=2)
-    slots = [jnp.max(jnp.where((grid > 0) & (rank == s), place[None], 0), axis=1) for s in range(CAP)]
-    table = jnp.stack(slots, axis=1).reshape(n_z, n_y, CAP)
-    table = jnp.take(table, (z - jnp.arange(n_z)) % n_z, axis=0)
-    table = table.transpose(1, 0, 2).reshape(n_y, n_z * CAP)
-    requests = jnp.pad(table, ((0, 0), (0, 128 - n_z * CAP)))[:, None, :]
-    flat = safe.reshape(-1, 1)
-    same = (flat // blocks == targets[None, :] // blocks) & (targets[None, :] < flat)
-    slot = jnp.minimum(jnp.sum(jnp.where(same, wanted[None, :], 0), axis=1), CAP - 1)
-    slot = slot.reshape(chosen.shape)
-    owner = safe // blocks
-    steps = z - owner // n_y
-    whole = (owner % n_y == y) & (steps >= 0) & (steps < NEAR)
-    inside = n_kv * CAP + steps * blocks + safe - owner * blocks
-    placed = jnp.where(whole, inside, owner * CAP + slot)
-    return requests, jnp.where(chosen < 0, -1, placed)
 
 
 def per_device(dims, tokens, chosen, query_weight, key_matrix, value_matrix, out_weight, out_gain):
@@ -598,18 +605,16 @@
     rows, width = tokens.shape
     blocks = rows // BLOCK_LENGTH
     heads_width = query_weight.shape[1]
-    requests, placed = index_tables(chosen, lax.axis_index("kv"), n_kv, n_y, blocks)
-    pair = jnp.concatenate([key_matrix, value_matrix], axis=1)
-    pair_width = pair.shape[1]
+    pair_width = key_matrix.shape[1] + value_matrix.shape[1]
     half_rows = rows // 2
     n_z = n_kv // n_y
     far = n_z - NEAR
     vmem, dma = pltpu.VMEM, pltpu.SemaphoreType.DMA
     bf16, f32, i32 = jnp.bfloat16, jnp.float32, jnp.int32
     in_vmem = pl.BlockSpec(memory_space=pltpu.VMEM)
-    return pl.pallas_call(
+    normed = pl.pallas_call(
         functools.partial(fused_kernel, dims),
-        out_shape=jax.ShapeDtypeStruct((half_rows, width), bf16),
+        out_shape=jax.ShapeDtypeStruct((half_rows, width), f32),
         in_specs=[
             pl.BlockSpec(memory_space=pltpu.SMEM),
             in_vmem,
@@ -621,6 +626,9 @@
         ],
         out_specs=in_vmem,
         scratch_shapes=[
+            vmem((blocks, 128), i32),
+            pltpu.SMEM((blocks, 128), i32),
+            vmem((n_y, 1, 128), i32),
             vmem((rows, width), bf16),
             vmem((width, pair_width), bf16),
             vmem((n_y * (1 + far), 1, 128), i32),
@@ -638,6 +646,7 @@
             vmem((half_rows, width), f32),
             vmem((half_rows, width), bf16),
             vmem((half_rows, width), bf16),
+            dma,
             dma,
             dma,
             dma((2,)),
@@ -660,7 +669,8 @@
             collective_id=0, has_side_effects=True, vmem_limit_bytes=60 * 1024 * 1024
         ),
         name="fused",
-    )(placed, requests, tokens, pair, query_weight, out_weight.T, out_gain[None, :])
+    )(chosen, chosen, tokens, key_matrix, value_matrix, query_weight, out_weight.T)
+    return (normed * out_gain[None, :]).astype(bf16)
 
 
 def solution(mesh):

time: 112 us -> 99.6 us (0.89)
  Pallas kernels: 103 us -> 96.6 us
  local copies, waits for them, and re-layouts: 4.78 us -> 0.01 us
  other arithmetic: 3.96 us -> 2.76 us
    pallas_call x1, Pallas kernels: 103 us -> 96.6 us  [per_device(): pl.pallas_call(functools.partial(fused_kernel, dims), out_shape=jax.Shape...]
    convert_element_type x1, other arithmetic: 0.01 us -> 2.76 us  [per_device(): return (normed * out_gain[None, :]).astype(bf16)]
    unnamed x1 -> x2, local copies, waits for them, and re-layouts: 2.3 us -> 0.01 us
    select_n x5 -> x0, other arithmetic: 1.41 us -> none  [the longest x1 1.31 us: index_tables(): return (requests, jnp.where(chosen < 0, -1, placed))]
    concatenate x1 -> x0, other arithmetic: 1.39 us -> none  [per_device(): pair = jnp.concatenate([key_matrix, value_matrix], axis=1)]
where the time goes in v3:
time: 99.6 us; the launch traced here: 99.3 us
  Pallas kernels  96.6 us (97%)
  other arithmetic  2.76 us (3%)
    pallas_call x1, Pallas kernels, per_device(): pl.pallas_call(functools.partial(fused_kernel, dims), out_shape=jax.Shape...  96.6 us
    convert_element_type x1, other arithmetic, per_device(): return (normed * out_gain[None, :]).astype(bf16)  2.76 us

profile of v3, /device:TPU:1, one launch (start us, length us, event | category | flops | bytes accessed | tf_op | source)
XLA Modules:
  0.0 99.3 jit_solution(3008039161048970101)
XLA Ops:
  0.0 0.0 copy-start
  0.0 96.6 %fused.1 = f32[256,2048]{1,0:T(8,128)} custom-call(s32[8,16]{1,0:T(8,128)} %chosen_rows.1, s32[8,16]{1,0:T(8,128)} %chosen_rows.1, bf16[512,2048]{1,0:T(8,128)(2,1)} %tokens_hbm.1, bf16[32,64]{1,0:T(8,128)(2,1)} %key_ref.1, bf16[32,64]{1,0:T(8,128)(2,1)} %value_ref.1, bf16[32,512]{1,0:T(8,128)(2,1)} %query_ref.1, bf16[32,512]{1,0:T(8,128)(2,1)} %bitcast.1), custom_call_target="tpu_custom_call" | custom-call | tf_op jit(solution)/shard_map/fused/pallas_call | solution.py:615
  96.6 0.0 copy-done
  96.6 2.8 %multiply_convert_fusion = bf16[256,2048]{1,0:T(8,128)(2,1)} fusion(f32[256,2048]{1,0:T(8,128)} %fused.1, f32[2048]{0:T(1024)S(1)} %copy-done), kind=kLoop, calls=%fused_computation | loop fusion | flops 1048576 | bytes 3153920 | tf_op jit(solution)/shard_map/convert_element_type | solution.py:673
Async XLA Ops:
  0.0 96.6 %copy-start = (f32[2048]{0:T(1024)S(1)}, f32[2048]{0:T(1024)}, u32[]{:S(2)}) copy-start(f32[2048]{0:T(1024)} %param.13) | copy-start | bytes 24580

commit v4 on v3

--- a/solution.py
+++ b/solution.py
@@ -31,6 +31,7 @@
     tokens,
     pair_all,
     requests_all,
+    far_requests,
     requests_smem,
     query_all,
     out_all,
@@ -45,6 +46,9 @@
     relayed,
     queries,
     gathered,
+    gathered1,
+    scores0,
+    scores1,
     attended,
     part_mine,
     part_send,
@@ -97,12 +101,18 @@
 
     barrier = pltpu.get_barrier_semaphore()
 
-    def greet(off, carry):
-        other = lax.rem(kv + off, n_kv)
-        pl.semaphore_signal(barrier, inc=1, device_id=(dp, other, tp), device_id_type=MESH)
-        return carry
-
-    lax.fori_loop(1, n_kv, greet, 0)
+    def row_mate(off):
+        return z * n_y + lax.rem(y + off, n_y)
+
+    def column_mate(off):
+        return lax.rem(z + off, n_z) * n_y + y
+
+    for off in range(1, n_y):
+        pl.semaphore_signal(barrier, inc=1, device_id=(dp, row_mate(off), tp), device_id_type=MESH)
+    for off in range(1, n_z):
+        pl.semaphore_signal(
+            barrier, inc=1, device_id=(dp, column_mate(off), tp), device_id_type=MESH
+        )
     for off in range(1, n_dp):
         pl.semaphore_signal(
             barrier, inc=1, device_id=(lax.rem(dp + off, n_dp), kv, tp), device_id_type=MESH
@@ -113,7 +123,7 @@
     my_cols = pl.ds(pl.multiple_of(dp * quarter, quarter), quarter)
     wide = jnp.float32
     pair = jnp.concatenate([key_ref[...].astype(wide), value_ref[...].astype(wide)], axis=1)
-    pair_all[my_rows, :] = pair.astype(jnp.bfloat16)
+    pair_all[z, y] = pair.astype(jnp.bfloat16).reshape(pair_all.shape[2:])
     query_all[my_rows, my_cols] = query_ref[:, my_cols]
     out_all[my_rows, my_cols] = out_ref[:, my_cols]
 
@@ -151,10 +161,44 @@
     to_placed = pltpu.make_async_copy(placed_vmem, placed_ref, place_sem)
     to_placed.start()
 
-    pl.semaphore_wait(barrier, n_kv - 1 + n_dp - 1 + 1)
+    pl.semaphore_wait(barrier, n_y - 1 + n_z - 1 + n_dp - 1 + 1)
+
+    def spread(piece, at, mate, count):
+        def one(off, carry):
+            remote(piece, piece, pair_sem.at[at], pair_sem.at[at + 1], dp, mate(off), tp).start()
+            return carry
+
+        lax.fori_loop(1, count, one, 0)
+
+    spread(pair_all.at[z, y, 0], 0, row_mate, n_y)
+    spread(pair_all.at[z, y, 1], 2, column_mate, n_z)
+
+    def ask_row(off, carry):
+        column = lax.rem(y + off, n_y)
+        remote(
+            requests_ref.at[pl.ds(column, 1)],
+            requests_all.at[pl.ds(y, 1)],
+            request_sem.at[0],
+            request_sem.at[1],
+            dp,
+            row_mate(off),
+            tp,
+        ).start()
+        return carry
+
+    lax.fori_loop(1, n_y, ask_row, 0)
+    for far in range(n_far):
+        remote(
+            requests_ref,
+            far_requests.at[far],
+            request_sem.at[2],
+            request_sem.at[3],
+            dp,
+            column_mate(n_z - near - far),
+            tp,
+        ).start()
 
     def send_row(off, carry):
-        other = z * n_y + lax.rem(y + off, n_y)
         for at, dst in enumerate((query_all, out_all)):
             remote(
                 dst.at[my_rows, my_cols],
@@ -162,47 +206,44 @@
                 y_sem.at[2 * at],
                 y_sem.at[2 * at + 1],
                 dp,
-                other,
+                row_mate(off),
                 tp,
             ).start()
         return carry
 
     lax.fori_loop(1, n_y, send_row, 0)
 
-    def send_pair(off, carry):
-        other = lax.rem(kv + off, n_kv)
-        mine = pair_all.at[my_rows, :]
-        remote(mine, mine, pair_sem.at[0], pair_sem.at[1], dp, other, tp).start()
+    pieces = pair_all.at[0, pl.ds(0, n_y - 1), 0]
+    bundles = pair_all.at[pl.ds(0, n_z - 1), :, 0]
+    drain(pieces, pair_sem.at[1])
+    spread(pair_all.at[z, :, 0], 4, column_mate, n_z)
+    drain(pieces, pair_sem.at[3])
+    spread(pair_all.at[:, y, 1], 6, row_mate, n_y)
+
+    near_asked = requests_all.at[pl.ds(0, n_y - 1)]
+    far_asked = requests_all.at[pl.ds(0, n_far * n_y)]
+    far_passed = requests_all.at[pl.ds(0, n_far * (n_y - 1))]
+    drain(far_asked, request_sem.at[3])
+
+    def pass_asked(off, carry):
+        column = lax.rem(y + off, n_y)
+        for far in range(n_far):
+            remote(
+                far_requests.at[far, pl.ds(column, 1)],
+                requests_all.at[pl.ds(n_y * (1 + far) + y, 1)],
+                request_sem.at[4],
+                request_sem.at[5],
+                dp,
+                row_mate(off),
+                tp,
+            ).start()
         return carry
 
-    lax.fori_loop(1, n_kv, send_pair, 0)
-
-    def ask(column, row, at):
-        remote(
-            requests_ref.at[pl.ds(column, 1)],
-            requests_all.at[pl.ds(at, 1)],
-            request_sem.at[0],
-            request_sem.at[1],
-            dp,
-            row * n_y + column,
-            tp,
-        ).start()
-
-    def ask_row(off, carry):
-        ask(lax.rem(y + off, n_y), z, y)
-        return carry
-
-    def ask_far(column, carry):
-        for far in range(n_far):
-            ask(column, lax.rem(z + n_z - near - far, n_z), n_y * (1 + far) + y)
-        return carry
-
-    lax.fori_loop(1, n_y, ask_row, 0)
-    lax.fori_loop(0, n_y, ask_far, 0)
-    asked = requests_all.at[pl.ds(0, n_y * (1 + n_far) - 1)]
-
-    others = pair_all.at[pl.ds(0, (n_kv - 1) * depth), :]
-    row_others = pair_all.at[pl.ds(0, (n_y - 1) * depth), :]
+    lax.fori_loop(1, n_y, pass_asked, 0)
+    for far in range(n_far):
+        requests_all[n_y * (1 + far) + y] = far_requests[far, y]
+
+    row_others = query_all.at[pl.ds(0, (n_y - 1) * depth), pl.ds(0, quarter)]
 
     above = lax.rem(z + 1, n_z) * n_y + y
     below = lax.rem(z + n_z - 1, n_z) * n_y + y
@@ -266,12 +307,15 @@
     cross(-1)
     cross(1)
 
-    drain(asked, request_sem.at[1])
+    drain(near_asked, request_sem.at[1])
+    drain(far_passed, request_sem.at[5])
     to_smem = pltpu.make_async_copy(requests_all, requests_smem, smem_sem)
     to_smem.start()
     load_tokens.wait()
-    drain(others, pair_sem.at[1])
-    pairs = jnp.dot(tokens[...], pair_all[...], preferred_element_type=jnp.float32)
+    drain(bundles, pair_sem.at[5])
+    drain(bundles, pair_sem.at[7])
+    weights = pair_all[...].reshape(tokens.shape[1], own.shape[2])
+    pairs = jnp.dot(tokens[...], weights, preferred_element_type=jnp.float32)
     pairs = pairs.astype(jnp.bfloat16).reshape(own.shape)
     own[...] = pairs
     pool[pl.ds(n_kv * CAP, blocks)] = pairs
@@ -471,8 +515,13 @@
             head = jnp.where(lane < HEAD_WIDTH, value, 0.0).astype(jnp.bfloat16)
             queries[:, 2 * d + side] = head.reshape(blocks, BLOCK_LENGTH, 2 * HEAD_WIDTH)
 
-    drain(others, pair_sem.at[0])
-    drain(asked, request_sem.at[0])
+    drain(pieces, pair_sem.at[0])
+    drain(pieces, pair_sem.at[2])
+    drain(bundles, pair_sem.at[4])
+    drain(bundles, pair_sem.at[6])
+    drain(near_asked, request_sem.at[0])
+    drain(far_asked, request_sem.at[2])
+    drain(far_passed, request_sem.at[4])
     drain(row_others, y_sem.at[0])
     drain(row_others, y_sem.at[2])
     for step in range(1, ups + 1):
@@ -538,38 +587,54 @@
     first_half = lane_at < BLOCK_LENGTH
     own_bias = jnp.where(lane_at <= lax.rem(row_at, BLOCK_LENGTH), 0.0, NEG)
 
-    def attend(block, carry):
+    def gather(block, keys_ref):
         shut = []
         for s in range(sel):
             at = placed_ref[block, s]
-            gathered[s * BLOCK_LENGTH : (s + 1) * BLOCK_LENGTH, :] = pool[jnp.maximum(at, 0)]
+            keys_ref[s * BLOCK_LENGTH : (s + 1) * BLOCK_LENGTH, :] = pool[jnp.maximum(at, 0)]
             shut.append(jnp.where(at < 0, NEG, 0.0))
         bias = [jnp.where(first_half, own_bias, shut[1])]
         for s in range(2, sel, 2):
             bias.append(jnp.where(first_half, shut[s], shut[s + 1]))
-        bias = jnp.concatenate(bias, axis=1)
-        keys = gathered[...]
-        outs = []
+        return jnp.concatenate(bias, axis=1)
+
+    def score(block, d, keys_ref, bias, scores_ref):
+        query_pair = queries[block, 2 * d : 2 * d + 2].reshape(pair_rows, 2 * HEAD_WIDTH)
+        scores = lax.dot_general(
+            query_pair, keys_ref[...], (((1,), (1,)), ((), ())), preferred_element_type=jnp.float32
+        )
+        scores_ref[d] = scores + bias
+
+    def soften(block, d, keys_ref, scores_ref):
+        scores = scores_ref[d]
+        expon = jnp.exp(scores - jnp.max(scores, axis=1, keepdims=True))
+        total = jnp.sum(expon, axis=1, keepdims=True)
+        mixed = jnp.dot(
+            expon.astype(jnp.bfloat16), keys_ref[...], preferred_element_type=jnp.float32
+        )
+        mixed = mixed * (1.0 / total)
+        even = pltpu.roll(mixed[:BLOCK_LENGTH], HEAD_WIDTH, 1)
+        both = jnp.where(first_half[:BLOCK_LENGTH], even, mixed[BLOCK_LENGTH:])
+        rows = pl.ds(pl.multiple_of(block * BLOCK_LENGTH, BLOCK_LENGTH), BLOCK_LENGTH)
+        attended[rows, d * 2 * HEAD_WIDTH : (d + 1) * 2 * HEAD_WIDTH] = both.astype(jnp.bfloat16)
+
+    def attend(pair, carry):
+        block = 2 * pair
+        ahead = jnp.minimum(block + 2, blocks - 1)
+        bias = gather(block + 1, gathered1)
         for d in range(n_dp):
-            query_pair = queries[block, 2 * d : 2 * d + 2].reshape(pair_rows, 2 * HEAD_WIDTH)
-            scores = lax.dot_general(
-                query_pair, keys, (((1,), (1,)), ((), ())), preferred_element_type=jnp.float32
-            )
-            scores = scores + bias
-            expon = jnp.exp(scores - jnp.max(scores, axis=1, keepdims=True))
-            total = jnp.sum(expon, axis=1, keepdims=True)
-            probs = expon.astype(jnp.bfloat16)
-            mixed = jnp.dot(probs, keys, preferred_element_type=jnp.float32) * (1.0 / total)
-            even = pltpu.roll(mixed[:BLOCK_LENGTH], HEAD_WIDTH, 1)
-            odd = mixed[BLOCK_LENGTH:]
-            outs.append(
-                jnp.where(first_half[:BLOCK_LENGTH], even, odd).astype(jnp.bfloat16)
-            )
-        rows = pl.ds(pl.multiple_of(block * BLOCK_LENGTH, BLOCK_LENGTH), BLOCK_LENGTH)
-        attended[rows, :] = jnp.concatenate(outs, axis=1)
+            score(block + 1, d, gathered1, bias, scores1)
+            soften(block, d, gathered, scores0)
+        bias = gather(ahead, gathered)
+        for d in range(n_dp):
+            score(ahead, d, gathered, bias, scores0)
+            soften(block + 1, d, gathered1, scores1)
         return carry
 
-    lax.fori_loop(0, blocks, attend, 0)
+    bias = gather(0, gathered)
+    for d in range(n_dp):
+        score(0, d, gathered, bias, scores0)
+    lax.fori_loop(0, blocks // 2, attend, 0)
 
     wait_across((2, 5))
 
@@ -630,8 +695,9 @@
             pltpu.SMEM((blocks, 128), i32),
             vmem((n_y, 1, 128), i32),
             vmem((rows, width), bf16),
-            vmem((width, pair_width), bf16),
+            vmem((n_z, n_y, 2, key_matrix.shape[0] // 2, pair_width), bf16),
             vmem((n_y * (1 + far), 1, 128), i32),
+            vmem((far, n_y, 1, 128), i32),
             pltpu.SMEM((n_y * (1 + far), 1, 128), i32),
             vmem((width, heads_width), bf16),
             vmem((width, heads_width), bf16),
@@ -642,6 +708,9 @@
             vmem((far, n_y, CAP, BLOCK_LENGTH, pair_width), bf16),
             vmem((blocks, heads_width // HEAD_WIDTH, BLOCK_LENGTH, pair_width), bf16),
             vmem((chosen.shape[1] * BLOCK_LENGTH, pair_width), bf16),
+            vmem((chosen.shape[1] * BLOCK_LENGTH, pair_width), bf16),
+            vmem((n_dp, 2 * BLOCK_LENGTH, chosen.shape[1] * BLOCK_LENGTH), f32),
+            vmem((n_dp, 2 * BLOCK_LENGTH, chosen.shape[1] * BLOCK_LENGTH), f32),
             vmem((rows, heads_width), bf16),
             vmem((half_rows, width), f32),
             vmem((half_rows, width), bf16),
@@ -649,8 +718,8 @@
             dma,
             dma,
             dma,
-            dma((2,)),
-            dma((2,)),
+            dma((8,)),
+            dma((6,)),
             dma((4,)),
             dma((2 * (n_z - 1),)),
             dma((2 * (n_z - 1),)),

time: 99.6 us -> 87.8 us (0.88)
  Pallas kernels: 96.6 us -> 84.8 us
    pallas_call x1, Pallas kernels: 96.6 us -> 84.8 us  [per_device(): pl.pallas_call(functools.partial(fused_kernel, dims), out_shape=jax.Shape...]
where the time goes in v4:
time: 87.8 us; the launch traced here: 87.5 us
  Pallas kernels  84.8 us (97%)
  other arithmetic  2.76 us (3%)
    pallas_call x1, Pallas kernels, per_device(): pl.pallas_call(functools.partial(fused_kernel, dims), out_shape=jax.Shape...  84.8 us
    convert_element_type x1, other arithmetic, per_device(): return (normed * out_gain[None, :]).astype(bf16)  2.76 us

profile of v4, /device:TPU:1, one launch (start us, length us, event | category | flops | bytes accessed | tf_op | source)
XLA Modules:
  0.0 87.5 jit_solution(17334026647570395289)
XLA Ops:
  0.0 0.0 copy-start
  0.0 84.8 %fused.1 = f32[256,2048]{1,0:T(8,128)} custom-call(s32[8,16]{1,0:T(8,128)} %chosen_rows.1, s32[8,16]{1,0:T(8,128)} %chosen_rows.1, bf16[512,2048]{1,0:T(8,128)(2,1)} %tokens_hbm.1, bf16[32,64]{1,0:T(8,128)(2,1)} %key_ref.1, bf16[32,64]{1,0:T(8,128)(2,1)} %value_ref.1, bf16[32,512]{1,0:T(8,128)(2,1)} %query_ref.1, bf16[32,512]{1,0:T(8,128)(2,1)} %bitcast.1), custom_call_target="tpu_custom_call" | custom-call | tf_op jit(solution)/shard_map/fused/pallas_call | solution.py:680
  84.8 0.0 copy-done
  84.8 2.8 %multiply_convert_fusion = bf16[256,2048]{1,0:T(8,128)(2,1)} fusion(f32[256,2048]{1,0:T(8,128)} %fused.1, f32[2048]{0:T(1024)S(1)} %copy-done), kind=kLoop, calls=%fused_computation | loop fusion | flops 1048576 | bytes 3153920 | tf_op jit(solution)/shard_map/convert_element_type | solution.py:742
Async XLA Ops:
  0.0 84.8 %copy-start = (f32[2048]{0:T(1024)S(1)}, f32[2048]{0:T(1024)}, u32[]{:S(2)}) copy-start(f32[2048]{0:T(1024)} %param.13) | copy-start | bytes 24580

commit v5 on v4

--- a/solution.py
+++ b/solution.py
@@ -277,15 +277,15 @@
         to = right if kind in (0, 2, 4) else left
         return remote(piece, piece, x_send.at[at], x_recv.at[at], to, kv, tp)
 
-    def cross(delta):
-        for kind in range(4):
-            across(delta, kind).start()
-
-    def cross_on(delta):
-        across(delta, 0).wait_recv()
-        across(delta, 4).start()
-        across(delta, 3).wait_recv()
-        across(delta, 5).start()
+    def cross(part, *deltas):
+        for delta in deltas:
+            across(delta, 2 * part).start()
+            across(delta, 2 * part + 1).start()
+
+    def cross_on(part, *deltas):
+        for delta in deltas:
+            across(delta, 3 * part).wait_recv()
+            across(delta, 4 + part).start()
 
     def start(copies):
         for copy in copies:
@@ -299,13 +299,14 @@
     drain(row_others, y_sem.at[3])
     start(ring(1, True))
     start(ring(1, False))
-    cross(0)
+    cross(0, 0)
+    cross(1, 0)
     arrive(ring(1, True))
     arrive(ring(1, False))
     start(ring(2, True))
     start(ring(2, False))
-    cross(-1)
-    cross(1)
+    cross(0, -1, 1)
+    cross_on(0, 0)
 
     drain(near_asked, request_sem.at[1])
     drain(far_passed, request_sem.at[5])
@@ -459,38 +460,42 @@
     for far in reversed(range(n_far)):
         send_far(far)
     share(0)
-    cross_on(0)
 
     arrive(ring(2, True))
     arrive(ring(2, False))
     start(ring(3, True))
-    cross(-2)
-    cross(2)
+    cross(0, -2, 2)
+    cross_on(0, -1, 1)
+    cross(1, -1, 1)
     pass_far(2)
     take_chain(1)
-    cross_on(-1)
-    cross_on(1)
+    cross_on(1, 0)
 
     arrive(ring(3, True))
     start(ring(4, True))
-    cross(-3)
+    cross(0, -3)
+    cross_on(0, -2, 2)
+    cross(1, -2, 2)
     pass_far(1)
     take_chain(2)
-    cross_on(-2)
+    cross_on(1, -1, 1)
 
     arrive(ring(4, True))
     start(ring(5, True))
-    cross(-4)
+    cross(0, -4)
+    cross_on(0, -3)
+    cross(1, -3)
     pass_far(0)
     take_chain(3)
-    cross_on(2)
-    cross_on(-3)
+    cross_on(1, -2, 2)
 
     arrive(ring(5, True))
-    cross(-5)
+    cross(0, -5)
+    cross_on(0, -4)
+    cross(1, -4)
     take_chain(4)
-    cross_on(-4)
-    cross_on(-5)
+    cross_on(0, -5)
+    cross(1, -5)
 
     def wait_across(kinds):
         def one(at, carry):
@@ -515,6 +520,7 @@
             head = jnp.where(lane < HEAD_WIDTH, value, 0.0).astype(jnp.bfloat16)
             queries[:, 2 * d + side] = head.reshape(blocks, BLOCK_LENGTH, 2 * HEAD_WIDTH)
 
+    cross_on(1, -3, -4, -5)
     drain(pieces, pair_sem.at[0])
     drain(pieces, pair_sem.at[2])
     drain(bundles, pair_sem.at[4])
@@ -618,44 +624,47 @@
         rows = pl.ds(pl.multiple_of(block * BLOCK_LENGTH, BLOCK_LENGTH), BLOCK_LENGTH)
         attended[rows, d * 2 * HEAD_WIDTH : (d + 1) * 2 * HEAD_WIDTH] = both.astype(jnp.bfloat16)
 
+    def turn(at):
+        return lax.rem(at + (1 - tp) * (blocks // 2), blocks)
+
     def attend(pair, carry):
-        block = 2 * pair
-        ahead = jnp.minimum(block + 2, blocks - 1)
-        bias = gather(block + 1, gathered1)
+        block, after = turn(2 * pair), turn(2 * pair + 1)
+        ahead = turn(jnp.minimum(2 * pair + 2, blocks - 1))
+        bias = gather(after, gathered1)
         for d in range(n_dp):
-            score(block + 1, d, gathered1, bias, scores1)
+            score(after, d, gathered1, bias, scores1)
             soften(block, d, gathered, scores0)
         bias = gather(ahead, gathered)
         for d in range(n_dp):
             score(ahead, d, gathered, bias, scores0)
-            soften(block + 1, d, gathered1, scores1)
+            soften(after, d, gathered1, scores1)
         return carry
 
-    bias = gather(0, gathered)
+    bias = gather(turn(0), gathered)
     for d in range(n_dp):
-        score(0, d, gathered, bias, scores0)
-    lax.fori_loop(0, blocks // 2, attend, 0)
+        score(turn(0), d, gathered, bias, scores0)
+    lax.fori_loop(0, blocks // 4, attend, 0)
 
     wait_across((2, 5))
 
+    rows_out = part_mine.shape[0]
+
+    def project(which):
+        rows = attended[pl.ds(pl.multiple_of(which * rows_out, rows_out), rows_out), :]
+        return lax.dot_general(
+            rows, out_all[...], (((1,), (1,)), ((), ())), preferred_element_type=jnp.float32
+        )
+
+    part_send[...] = project(1 - tp).astype(jnp.bfloat16)
+    swap = remote(part_send, part_recv, half_sem.at[0], half_sem.at[1], dp, kv, 1 - tp)
+    swap.start()
+    lax.fori_loop(blocks // 4, blocks // 2, attend, 0)
     def drain_across(at, carry):
         for kind in range(6):
             across(at - z, kind).wait_send()
         return carry
 
     lax.fori_loop(0, n_z, drain_across, 0)
-
-    rows_out = part_mine.shape[0]
-
-    def project(which):
-        rows = attended[pl.ds(pl.multiple_of(which * rows_out, rows_out), rows_out), :]
-        return lax.dot_general(
-            rows, out_all[...], (((1,), (1,)), ((), ())), preferred_element_type=jnp.float32
-        )
-
-    part_send[...] = project(1 - tp).astype(jnp.bfloat16)
-    swap = remote(part_send, part_recv, half_sem.at[0], half_sem.at[1], dp, kv, 1 - tp)
-    swap.start()
     part_mine[...] = project(tp)
     swap.wait_recv()
     mixed = part_mine[...] + part_recv[...].astype(jnp.float32)

time: 87.8 us -> 85 us (0.968)
  Pallas kernels: 84.8 us -> 81.8 us
    pallas_call x1, Pallas kernels: 84.8 us -> 81.8 us  [per_device(): pl.pallas_call(functools.partial(fused_kernel, dims), out_shape=jax.Shape...]
where the time goes in v5:
time: 85 us; the launch traced here: 84.6 us
  Pallas kernels  81.8 us (96%)
  other arithmetic  2.76 us (3%)
    pallas_call x1, Pallas kernels, per_device(): pl.pallas_call(functools.partial(fused_kernel, dims), out_shape=jax.Shape...  81.8 us
    convert_element_type x1, other arithmetic, per_device(): return (normed * out_gain[None, :]).astype(bf16)  2.76 us

profile of v5, /device:TPU:1, one launch (start us, length us, event | category | flops | bytes accessed | tf_op | source)
XLA Modules:
  0.0 84.6 jit_solution(7672307569980953373)
XLA Ops:
  0.0 0.0 copy-start
  0.0 81.8 %fused.1 = f32[256,2048]{1,0:T(8,128)} custom-call(s32[8,16]{1,0:T(8,128)} %chosen_rows.1, s32[8,16]{1,0:T(8,128)} %chosen_rows.1, bf16[512,2048]{1,0:T(8,128)(2,1)} %tokens_hbm.1, bf16[32,64]{1,0:T(8,128)(2,1)} %key_ref.1, bf16[32,64]{1,0:T(8,128)(2,1)} %value_ref.1, bf16[32,512]{1,0:T(8,128)(2,1)} %query_ref.1, bf16[32,512]{1,0:T(8,128)(2,1)} %bitcast.1), custom_call_target="tpu_custom_call" | custom-call | tf_op jit(solution)/shard_map/fused/pallas_call | solution.py:689
  81.8 0.0 copy-done
  81.8 2.8 %multiply_convert_fusion = bf16[256,2048]{1,0:T(8,128)(2,1)} fusion(f32[256,2048]{1,0:T(8,128)} %fused.1, f32[2048]{0:T(1024)S(1)} %copy-done), kind=kLoop, calls=%fused_computation | loop fusion | flops 1048576 | bytes 3153920 | tf_op jit(solution)/shard_map/convert_element_type | solution.py:751
Async XLA Ops:
  0.0 81.8 %copy-start = (f32[2048]{0:T(1024)S(1)}, f32[2048]{0:T(1024)}, u32[]{:S(2)}) copy-start(f32[2048]{0:T(1024)} %param.13) | copy-start | bytes 24580
